TPU v7x, 32 devices: a whole 2x2x4 slice. The times are simulated.
32 devices in a mesh: sp: 16 (over z, y, x), tp: 2 (over core).
Axes of the slice: x: 2, y: 2, z: 4, core: 2. Of those that a mesh axis runs over, the one named last changes fastest.
Arguments:
- stream: bfloat16 [2048, 2048], P('sp'), may hold values from -6 to 6
- query_narrow: bfloat16 [2048, 512], P('sp', 'tp'), may hold values from -7 to 7
- query_broad: bfloat16 [2048, 1024], P('sp', 'tp'), may hold values from -7 to 7
- key_narrow: bfloat16 [2048, 512], P('sp', 'tp'), may hold values from -7 to 7
- key_broad: bfloat16 [2048, 1024], P('sp', 'tp'), may hold values from -7 to 7
- value_narrow: bfloat16 [2048, 512], P('sp', 'tp'), may hold values from -6 to 6
- value_broad: bfloat16 [2048, 1024], P('sp', 'tp'), may hold values from -6 to 6
- key_offsets: float32 [2048, 16], P('sp', 'tp'), may hold values from -20 to 0
- out_narrow: bfloat16 [512, 2048], P('tp'), may hold values from -0.4375 to 0.4375
- out_broad: bfloat16 [1024, 2048], P('tp'), may hold values from -0.4375 to 0.4375
- norm_gain: float32 [2048], replicated, may hold values from 0.1 to 1.9
- gate_weight: bfloat16 [2048, 3072], P('sp', 'tp'), may hold values from -0.125 to 0.125
- up_weight: bfloat16 [2048, 3072], P('sp', 'tp'), may hold values from -0.125 to 0.125
- down_weight: bfloat16 [3072, 2048], P('tp', 'sp'), may hold values from -0.21875 to 0.21875
Outputs:
- result: bfloat16 [2048, 2048], P(('sp', 'tp'))
All inputs are finite; a program needn't handle non-finite values.
Results may differ from a plain program's by a relative error of at most 0.028.
Values may be sent and summed in bfloat16 or wider, within the bound.
No kernel may reach another device: no remote copies, remote signals or barrier semaphores. Data moves between devices by JAX's collectives and lax.ppermute only.
A program may use at most 64 MiB of HBM per device.

v0:
```python
import jax
import jax.numpy as jnp
from jax import lax
from jax.sharding import PartitionSpec as P

NARROW_SIZE = 64
BROAD_SIZE = 128


grain = 8
block_keys = 512
norm_eps = 1e-06


def block_plan(length):
    return (length // block_keys, block_keys)


def slice_rows(array, first, count):
    return lax.dynamic_slice_in_dim(array, first, count, 0)


def head_logs(queries, keys_block, offset_block, positions, key_positions, scale):
    logits = (
        jnp.einsum("qhd,khd->hqk", queries, keys_block, preferred_element_type=jnp.float32) * scale
    )
    logits = logits + jnp.transpose(offset_block)[:, None, :]
    causal = (key_positions[None, :] < positions[:, None])[None, :, :]
    lognot = jnp.where(causal, jax.nn.log_sigmoid(-logits), 0.0)
    return (logits, causal, lognot)


def sub_totals(lognot):
    heads, count, length = lognot.shape
    return lognot.reshape(heads, count, length // grain, grain).sum(axis=3)


def weighted_values(logits, causal, lognot, after, values):
    heads, count, length = lognot.shape
    grouped = lognot.reshape(heads, count, length // grain, grain)
    within = lax.cumsum(grouped, axis=3, reverse=True) - grouped
    later = (within + after[:, :, :, None]).reshape(heads, count, length)
    weights = jnp.where(causal, jnp.exp(jax.nn.log_sigmoid(logits) + later), 0.0).astype(
        jnp.bfloat16
    )
    return jnp.einsum("hqk,khd->qhd", weights, values, preferred_element_type=jnp.float32)


def local(
    stream,
    query_narrow,
    query_broad,
    key_narrow,
    key_broad,
    value_narrow,
    value_broad,
    key_offsets,
    out_narrow,
    out_broad,
    norm_gain,
    gate_weight,
    up_weight,
    down_weight,
):
    rows = stream.shape[0]
    heads = query_narrow.shape[1] // NARROW_SIZE
    shaped_narrow = query_narrow.reshape(rows, heads, NARROW_SIZE)
    shaped_broad = query_broad.reshape(rows, heads, BROAD_SIZE)
    positions = lax.axis_index("sp") * rows + jnp.arange(rows, dtype=jnp.int32)
    scale_narrow = NARROW_SIZE ** (-0.5)
    scale_broad = BROAD_SIZE ** (-0.5)

    def key_block(keys_narrow, keys_broad, offsets, first, count):
        block_narrow = slice_rows(keys_narrow, first, count).reshape(count, heads, NARROW_SIZE)
        block_broad = slice_rows(keys_broad, first, count).reshape(count, heads, BROAD_SIZE)
        pairs = slice_rows(offsets, first, count).reshape(count, heads, 2)
        return (block_narrow, block_broad, pairs[:, :, 0], pairs[:, :, 1])

    def value_block(values_narrow, values_broad, first, count):
        return (
            slice_rows(values_narrow, first, count).reshape(count, heads, NARROW_SIZE),
            slice_rows(values_broad, first, count).reshape(count, heads, BROAD_SIZE),
        )

    empty_narrow = jnp.zeros((rows, heads, NARROW_SIZE), jnp.float32)
    empty_broad = jnp.zeros((rows, heads, BROAD_SIZE), jnp.float32)
    total_subs = rows * lax.axis_size("sp") // grain
    zeros_subs = jnp.zeros((heads, rows, total_subs), jnp.float32)
    keys_narrow = lax.all_gather(key_narrow, "sp", axis=0, tiled=True)
    keys_broad = lax.all_gather(key_broad, "sp", axis=0, tiled=True)
    offsets = lax.all_gather(key_offsets.astype(jnp.bfloat16), "sp", axis=0, tiled=True).astype(
        jnp.float32
    )
    steps, span = block_plan(keys_narrow.shape[0])

    def count_one_step(index, sums):
        first = index * span
        block_narrow, block_broad, offset_narrow, offset_broad = key_block(
            keys_narrow, keys_broad, offsets, first, span
        )
        key_positions = first + jnp.arange(span, dtype=jnp.int32)
        slot = first // grain
        lognot_narrow = head_logs(
            shaped_narrow, block_narrow, offset_narrow, positions, key_positions, scale_narrow
        )[2]
        lognot_broad = head_logs(
            shaped_broad, block_broad, offset_broad, positions, key_positions, scale_broad
        )[2]
        return (
            lax.dynamic_update_slice(sums[0], sub_totals(lognot_narrow), (0, 0, slot)),
            lax.dynamic_update_slice(sums[1], sub_totals(lognot_broad), (0, 0, slot)),
        )

    sums_narrow, sums_broad = lax.fori_loop(0, steps, count_one_step, (zeros_subs, zeros_subs))
    after_narrow = lax.cumsum(sums_narrow, axis=2, reverse=True) - sums_narrow
    after_broad = lax.cumsum(sums_broad, axis=2, reverse=True) - sums_broad
    value_keys_narrow = lax.all_gather(key_narrow, "sp", axis=0, tiled=True)
    value_keys_broad = lax.all_gather(key_broad, "sp", axis=0, tiled=True)
    values_narrow = lax.all_gather(value_narrow, "sp", axis=0, tiled=True)
    values_broad = lax.all_gather(value_broad, "sp", axis=0, tiled=True)
    value_offsets = lax.all_gather(
        key_offsets.astype(jnp.bfloat16), "sp", axis=0, tiled=True
    ).astype(jnp.float32)
    steps, value_span = block_plan(value_keys_narrow.shape[0])

    def value_one_step(index, sums):
        first = index * value_span
        block_narrow, block_broad, offset_narrow, offset_broad = key_block(
            value_keys_narrow, value_keys_broad, value_offsets, first, value_span
        )
        held_narrow, held_broad = value_block(values_narrow, values_broad, first, value_span)
        key_positions = first + jnp.arange(value_span, dtype=jnp.int32)
        slot = first // grain
        logits_narrow, causal_narrow, lognot_narrow = head_logs(
            shaped_narrow, block_narrow, offset_narrow, positions, key_positions, scale_narrow
        )
        logits_broad, causal_broad, lognot_broad = head_logs(
            shaped_broad, block_broad, offset_broad, positions, key_positions, scale_broad
        )
        later_narrow = lax.dynamic_slice_in_dim(after_narrow, slot, value_span // grain, 2)
        later_broad = lax.dynamic_slice_in_dim(after_broad, slot, value_span // grain, 2)
        return (
            sums[0]
            + weighted_values(
                logits_narrow, causal_narrow, lognot_narrow, later_narrow, held_narrow
            ),
            sums[1]
            + weighted_values(logits_broad, causal_broad, lognot_broad, later_broad, held_broad),
        )

    acc_narrow, acc_broad = lax.fori_loop(0, steps, value_one_step, (empty_narrow, empty_broad))
    attended_narrow = acc_narrow.reshape(rows, heads * NARROW_SIZE).astype(jnp.bfloat16)
    attended_broad = acc_broad.reshape(rows, heads * BROAD_SIZE).astype(jnp.bfloat16)
    share = rows // lax.axis_size("tp")
    own = lax.axis_index("tp") * share
    first = jnp.int32(0)
    summed = lax.psum_scatter(
        (
            jnp.dot(
                slice_rows(attended_narrow, first, share * lax.axis_size("tp")),
                out_narrow,
                preferred_element_type=jnp.float32,
            )
            + jnp.dot(
                slice_rows(attended_broad, first, share * lax.axis_size("tp")),
                out_broad,
                preferred_element_type=jnp.float32,
            )
        ).astype(jnp.bfloat16),
        "tp",
        scatter_dimension=0,
        tiled=True,
    ).astype(jnp.float32)
    mid_own = (slice_rows(stream, own, share).astype(jnp.float32) + summed).astype(jnp.bfloat16)
    middle = mid_own.astype(jnp.float32)
    scaled = middle * lax.rsqrt(jnp.mean(middle * middle, axis=1, keepdims=True) + norm_eps)
    normed = lax.all_gather((scaled * norm_gain).astype(jnp.bfloat16), "tp", axis=0, tiled=True)
    part_gate = lax.all_gather(gate_weight, "sp", axis=0, tiled=True)
    part_up = lax.all_gather(up_weight, "sp", axis=0, tiled=True)
    gate = jnp.dot(normed, part_gate, preferred_element_type=jnp.float32)
    up = jnp.dot(normed, part_up, preferred_element_type=jnp.float32)
    hidden = (jax.nn.silu(gate) * up).astype(jnp.bfloat16)
    down_full = lax.all_gather(down_weight, "sp", axis=1, tiled=True)
    mixed = lax.psum_scatter(
        jnp.dot(
            slice_rows(hidden, jnp.int32(0), share * lax.axis_size("tp")),
            down_full,
            preferred_element_type=jnp.float32,
        ).astype(jnp.bfloat16),
        "tp",
        scatter_dimension=0,
        tiled=True,
    ).astype(jnp.float32)
    return (mid_own.astype(jnp.float32) + mixed).astype(jnp.bfloat16)


def solution(mesh):
    placed = (
        P("sp", None),
        P("sp", "tp"),
        P("sp", "tp"),
        P("sp", "tp"),
        P("sp", "tp"),
        P("sp", "tp"),
        P("sp", "tp"),
        P("sp", "tp"),
        P("tp", None),
        P("tp", None),
        P(),
        P("sp", "tp"),
        P("sp", "tp"),
        P("tp", "sp"),
    )
    return jax.shard_map(
        local, mesh=mesh, in_specs=placed, out_specs=P(("sp", "tp"), None), check_vma=False
    )
```

profile of v0, /device:TPU:24, one launch (start us, length us, event | category | flops | bytes accessed | tf_op | source)
XLA Modules:
  0.0 1449.8 jit_solution(2472093632499235351)
XLA Ops:
  15.9 32.7 %all_gather.32 = bf16[2048,8]{0,1:T(8,128)(2,1)S(1)} all-gather(bf16[128,8]{0,1:T(8,128)(2,1)S(1)} %convert_element_type.72), channel_id=1, replica_groups=mesh['sp'=16,'tp'=2] {'sp'}, dimensions={0}, use_global_device_ids=true | all-gather | bytes 34816 | tf_op jit(solution)/shard_map/all_gather | solution.py:121
  50.2 10.7 all-gather.10.cloned.1.call-done
  60.9 64.3 %all-gather.12.cloned.1.call-done = bf16[2048,512]{0,1:T(8,128)(2,1)} async-done(((bf16[128,512]{0,1:T(8,128)(2,1)}), bf16[2048,512]{0,1:T(8,128)(2,1)}) %all-gather.12.cloned.1.call-update) | async-done | bytes 2097168 | tf_op jit(solution)/shard_map/all_gather | solution.py:118
  125.3 28.6 %while.36 = (s32[]{:T(128)}, f32[4,128,256]{1,2,0:T(8,128)S(1)}, f32[4,128,256]{1,2,0:T(8,128)S(1)}, bf16[2048,256]{0,1:T(8,128)(2,1)}, bf16[128,4,64]{0,2,1:T(8...) while((s32[]{:T(128)}, f32[4,128,256]{1,2,0:T(8,128)S(1)}, ...), condition=%wide.region_3.4_spmd.clone, body=%wide.region_0.3_spmd.clone.sunk | while | flops 106431104 | bytes 3691926 | solution.py:114
  154.0 4.6 fusion.50
  161.5 4.6 fusion.48
  170.3 7.6 all-gather.8.cloned.1.call-done
  177.9 64.2 %all-gather.14.cloned.1.call-done = bf16[2048,512]{0,1:T(8,128)(2,1)} async-done(((bf16[128,512]{0,1:T(8,128)(2,1)}), bf16[2048,512]{0,1:T(8,128)(2,1)}) %all-gather.14.cloned.1.call-update) | async-done | bytes 2097168 | tf_op jit(solution)/shard_map/all_gather | solution.py:120
  242.1 863.7 %while.37 = (s32[]{:T(128)}, f32[128,4,64]{0,2,1:T(8,128)}, f32[128,4,128]{0,2,1:T(8,128)}, bf16[2048,256]{0,1:T(8,128)(2,1)}, bf16[2048,256]{0,1:T(8,128)(2,1)}...) while((s32[]{:T(128)}, f32[128,4,64]{0,2,1:T(8,128)}, ...), condition=%wide.region_11.12_spmd.clone, body=%wide.region_8.11_spmd.clone.sunk | while | flops 221512320 | bytes 29971964 | solution.py:151
  270.3 96.6 %reduce_window_sum.71 = f32[4,128,64,8]{1,3,2,0:T(8,128)} reduce-window(f32[4,128,64,8]{1,3,2,0:T(8,128)} %get-tuple-element.879, f32[]{:T(128)} %constant.262.clone.1..sunk), window={size=1x1x1x8 pad=0_0x0_0x0_0x0_7}, to_apply=%region_10.10 | reduce-window | flops 1835008 | bytes 2097156 | tf_op jit(solution)/shard_map/while/body/eval_jaxpr/reduce_window_sum | solution.py:41
  368.5 4.1 fusion.118
  372.6 95.5 %reduce_window_sum.70 = f32[4,128,64,8]{1,3,2,0:T(8,128)} reduce-window(f32[4,128,64,8]{1,3,2,0:T(8,128)S(1)} %get-tuple-element.876, f32[]{:T(128)} %constant.262.clone.1..sunk), window={size=1x1x1x8 pad=0_0x0_0x0_0x0_7}, to_apply=%region_9.9 | reduce-window | flops 1835008 | bytes 2097156 | tf_op jit(solution)/shard_map/while/body/eval_jaxpr/reduce_window_sum | solution.py:41
  468.1 3.8 fusion.117
  481.4 96.6 %reduce_window_sum.71 = f32[4,128,64,8]{1,3,2,0:T(8,128)} reduce-window(f32[4,128,64,8]{1,3,2,0:T(8,128)} %get-tuple-element.879, f32[]{:T(128)} %constant.262.clone.1..sunk), window={size=1x1x1x8 pad=0_0x0_0x0_0x0_7}, to_apply=%region_10.10 | reduce-window | flops 1835008 | bytes 2097156 | tf_op jit(solution)/shard_map/while/body/eval_jaxpr/reduce_window_sum | solution.py:41
  579.7 4.1 fusion.118
  583.8 95.5 %reduce_window_sum.70 = f32[4,128,64,8]{1,3,2,0:T(8,128)} reduce-window(f32[4,128,64,8]{1,3,2,0:T(8,128)S(1)} %get-tuple-element.876, f32[]{:T(128)} %constant.262.clone.1..sunk), window={size=1x1x1x8 pad=0_0x0_0x0_0x0_7}, to_apply=%region_9.9 | reduce-window | flops 1835008 | bytes 2097156 | tf_op jit(solution)/shard_map/while/body/eval_jaxpr/reduce_window_sum | solution.py:41
  679.3 3.9 fusion.117
  692.6 96.6 %reduce_window_sum.71 = f32[4,128,64,8]{1,3,2,0:T(8,128)} reduce-window(f32[4,128,64,8]{1,3,2,0:T(8,128)} %get-tuple-element.879, f32[]{:T(128)} %constant.262.clone.1..sunk), window={size=1x1x1x8 pad=0_0x0_0x0_0x0_7}, to_apply=%region_10.10 | reduce-window | flops 1835008 | bytes 2097156 | tf_op jit(solution)/shard_map/while/body/eval_jaxpr/reduce_window_sum | solution.py:41
  790.9 4.2 fusion.118
  795.0 95.5 %reduce_window_sum.70 = f32[4,128,64,8]{1,3,2,0:T(8,128)} reduce-window(f32[4,128,64,8]{1,3,2,0:T(8,128)S(1)} %get-tuple-element.876, f32[]{:T(128)} %constant.262.clone.1..sunk), window={size=1x1x1x8 pad=0_0x0_0x0_0x0_7}, to_apply=%region_9.9 | reduce-window | flops 1835008 | bytes 2097156 | tf_op jit(solution)/shard_map/while/body/eval_jaxpr/reduce_window_sum | solution.py:41
  890.5 3.9 fusion.117
  903.8 96.6 %reduce_window_sum.71 = f32[4,128,64,8]{1,3,2,0:T(8,128)} reduce-window(f32[4,128,64,8]{1,3,2,0:T(8,128)} %get-tuple-element.879, f32[]{:T(128)} %constant.262.clone.1..sunk), window={size=1x1x1x8 pad=0_0x0_0x0_0x0_7}, to_apply=%region_10.10 | reduce-window | flops 1835008 | bytes 2097156 | tf_op jit(solution)/shard_map/while/body/eval_jaxpr/reduce_window_sum | solution.py:41
  1002.1 4.1 fusion.118
  1006.2 95.5 %reduce_window_sum.70 = f32[4,128,64,8]{1,3,2,0:T(8,128)} reduce-window(f32[4,128,64,8]{1,3,2,0:T(8,128)S(1)} %get-tuple-element.876, f32[]{:T(128)} %constant.262.clone.1..sunk), window={size=1x1x1x8 pad=0_0x0_0x0_0x0_7}, to_apply=%region_9.9 | reduce-window | flops 1835008 | bytes 2097156 | tf_op jit(solution)/shard_map/while/body/eval_jaxpr/reduce_window_sum | solution.py:41
  1101.7 3.9 fusion.117
  1112.8 6.2 reduce-scatter.3.cloned.1.call-done
  1122.5 92.0 %all-gather.16.cloned.1.call-done = bf16[2048,1536]{1,0:T(8,128)(2,1)} async-done(((bf16[128,1536]{1,0:T(8,128)(2,1)}), bf16[2048,1536]{1,0:T(8,128)(2,1)}) %all-gather.16.cloned.1.call-update) | async-done | bytes 6291472 | tf_op jit(solution)/shard_map/all_gather | solution.py:178
  1214.5 4.7 fusion.57
  1219.2 90.1 %all-gather.18.cloned.1.call-done = bf16[2048,1536]{1,0:T(8,128)(2,1)} async-done(((bf16[128,1536]{1,0:T(8,128)(2,1)}), bf16[2048,1536]{1,0:T(8,128)(2,1)}) %all-gather.18.cloned.1.call-update) | async-done | bytes 6291472 | tf_op jit(solution)/shard_map/all_gather | solution.py:179
  1309.2 115.9 %all-gather.20.cloned.1.call-done = bf16[1536,2048]{1,0:T(8,128)(2,1)} async-done(((bf16[1536,128]{1,0:T(8,128)(2,1)}), bf16[1536,2048]{1,0:T(8,128)(2,1)}) %all-gather.20.cloned.1.call-update) | async-done | bytes 6291472 | tf_op jit(solution)/shard_map/all_gather | solution.py:183
  1425.1 7.7 convolution_convert_fusion
  1432.8 8.4 reduce-scatter.5.cloned.1.call-done
  (181 shorter events, 102.3 us)
Async XLA Ops:
  6.5 1102.8 %copy-start = (bf16[512,2048]{1,0:T(8,128)(2,1)S(1)}, bf16[512,2048]{1,0:T(8,128)(2,1)}, u32[]{:S(2)}) copy-start(bf16[512,2048]{1,0:T(8,128)(2,1)} %param.27) | copy-start | bytes 6291460
  6.5 54.4 %all-gather.10.cloned.1.call-start = ((), (), s32[]{:S(2)}) async-start(), calls=%async_computation.3 | async-start | bytes 1114112 | tf_op jit(solution)/shard_map/all_gather | solution.py:117
  8.3 117.0 %all-gather.12.cloned.1.call-start = ((), (), s32[]{:S(2)}) async-start(), calls=%async_computation.4 | async-start | bytes 2228224 | tf_op jit(solution)/shard_map/all_gather | solution.py:118
  10.0 167.9 %all-gather.8.cloned.1.call-start = ((), (), s32[]{:S(2)}) async-start(), calls=%async_computation.2 | async-start | bytes 1114112 | tf_op jit(solution)/shard_map/all_gather | solution.py:119
  11.6 230.5 %all-gather.14.cloned.1.call-start = ((), (), s32[]{:S(2)}) async-start(), calls=%async_computation.5 | async-start | bytes 2228224 | tf_op jit(solution)/shard_map/all_gather | solution.py:120
  13.4 1105.6 %reduce-scatter.3.cloned.1.call-start = ((), (), s32[]{:S(2)}) async-start(), calls=%async_computation.6 | async-start | bytes 786432 | tf_op jit(solution)/shard_map/reduce_scatter | solution.py:157
  158.6 0.8 copy-start.3
  166.1 0.8 copy-start.4
  265.1 5.2 copy-start.2
  267.1 1.0 copy-start.1
  476.2 5.2 copy-start.2
  478.2 1.0 copy-start.1
  687.4 5.2 copy-start.2
  689.4 1.0 copy-start.1
  898.7 5.2 copy-start.2
  900.6 1.0 copy-start.1
  1105.8 13.2 copy-start.5
  1105.8 14.4 copy-start.6
  1110.6 103.9 %all-gather.16.cloned.1.call-start = ((), (), s32[]{:S(2)}) async-start(), calls=%async_computation.7 | async-start | bytes 6684672 | tf_op jit(solution)/shard_map/all_gather | solution.py:178
  1111.2 198.0 %all-gather.18.cloned.1.call-start = ((), (), s32[]{:S(2)}) async-start(), calls=%async_computation.8 | async-start | bytes 6684672 | tf_op jit(solution)/shard_map/all_gather | solution.py:179
  1112.0 313.2 %all-gather.20.cloned.1.call-start = ((), (), s32[]{:S(2)}) async-start(), calls=%async_computation.9 | async-start | bytes 6684672 | tf_op jit(solution)/shard_map/all_gather | solution.py:183
  1112.7 328.5 %reduce-scatter.5.cloned.1.call-start = ((), (), s32[]{:S(2)}) async-start(), calls=%async_computation.10 | async-start | bytes 786432 | tf_op jit(solution)/shard_map/reduce_scatter | solution.py:184
Sparse Core Ops, SparseCore 0:
  10.0 50.8 all-gather.9
  63.6 61.5 all-gather.11
  128.0 49.9 all-gather.7
  180.5 61.6 all-gather.13
  1110.8 8.1 reduce-scatter.2
  1121.6 92.8 all-gather.15
  1217.3 91.9 all-gather.17
  1311.9 113.1 all-gather.19
  1432.9 8.1 reduce-scatter.4
where the time goes:
time: 1460 us; the launch traced here: 1450 us
  other arithmetic  798 us (55%)
  waiting for transfers between devices  461 us (32%)
  matrix products  67.9 us (5%)
  local copies, waits for them, and re-layouts  53.3 us (4%)
  blocking collectives  34.9 us (2%)
  loops' own time  20 us (1%)
    another operation x8, other arithmetic, weighted_values(): within = lax.cumsum(grouped, axis=3, reverse=True) - grouped  768 us
    all_gather x1, waiting for transfers between devices, local(): down_full = lax.all_gather(down_weight, 'sp', axis=1, tiled=True)  116 us
    all_gather x1, waiting for transfers between devices, local(): part_gate = lax.all_gather(gate_weight, 'sp', axis=0, tiled=True)  92 us
    all_gather x1, waiting for transfers between devices, local(): part_up = lax.all_gather(up_weight, 'sp', axis=0, tiled=True)  90.1 us
    all_gather x1, waiting for transfers between devices, local(): value_keys_broad = lax.all_gather(key_broad, 'sp', axis=0, tiled=True)  64.3 us
    all_gather x1, waiting for transfers between devices, local(): values_broad = lax.all_gather(value_broad, 'sp', axis=0, tiled=True)  64.2 us
    all_gather x1, blocking collectives, local(): lax.all_gather(key_offsets.astype(jnp.bfloat16), 'sp', axis=0, tiled=True)  32.7 us
    dot_general x8, matrix products, weighted_values(): jnp.einsum('hqk,khd->qhd', weights, values, preferred_element_type=jnp.fl...  31.9 us
  transfers between devices with their start and end apart: 9, of which 9 were waited for; matrix products, arithmetic and copies ran while one was open for 4% of the time, Pallas kernels for 0%

commit v1 on v0

v1 whole, which is shorter than its diff:
```python
import functools
import math

import jax
import jax.numpy as jnp
from jax import lax
from jax.experimental import pallas as pl
from jax.experimental.pallas import tpu as pltpu
from jax.sharding import PartitionSpec as P

NARROW_SIZE = 64
BROAD_SIZE = 128
LANES = 128
EXTRA = 8
KV_LANES = 2 * BROAD_SIZE + 2 * NARROW_SIZE
ALL_LANES = KV_LANES + BROAD_SIZE + 2 * NARROW_SIZE
norm_eps = 1e-06
NEG = -1e30
BF = jnp.bfloat16
F32 = jnp.float32
ANY = pl.BlockSpec(memory_space=pl.ANY)
VMEM = pl.BlockSpec(memory_space=pltpu.VMEM)
SMEM = pl.BlockSpec(memory_space=pltpu.SMEM)

TEAM_BITS = (0, 2)
PEER_BITS = (1, 3)


class Plan:
    def __init__(self, sp, tp, heads, hidden):
        self.sp, self.tp = sp, tp
        self.split = sp == 16 and heads % 4 == 0 and hidden % (4 * LANES) == 0
        self.team_bits = TEAM_BITS if self.split else ()
        self.peer_bits = PEER_BITS if self.split else ()
        self.team = 4 if self.split else 1
        self.peers = sp // self.team

    def place(self, value, bits):
        out = 0
        for j, bit in enumerate(bits):
            out = out + (((value >> j) & 1) << bit)
        return out

    def index(self, t, w):
        if not self.split:
            return w
        return self.place(t, self.team_bits) + self.place(w, self.peer_bits)

    def member(self, i):
        if not self.split:
            return i * 0
        return sum(((i >> bit) & 1) << j for j, bit in enumerate(self.team_bits))

    def peer(self, i):
        if not self.split:
            return i
        return sum(((i >> bit) & 1) << j for j, bit in enumerate(self.peer_bits))

    def swap(self, array, offset):
        return lax.ppermute(array, "sp", [(i, i ^ offset) for i in range(self.sp)])

    def team_swap(self, array, r):
        return self.swap(array, self.place(r, self.team_bits))

    def peer_swap(self, array, r):
        return self.swap(array, self.place(r, self.peer_bits))


def pick(array, index):
    return lax.dynamic_index_in_dim(array, index, 0, keepdims=False)


def cost(flops, moved, transcendentals=0):
    return pl.CostEstimate(
        flops=int(flops), bytes_accessed=int(moved), transcendentals=int(transcendentals)
    )


def attention_kernel(plan, me_ref, own_ref, *refs):
    team, rows = plan.team, own_ref.shape[2] - EXTRA
    local_heads = own_ref.shape[1]
    part_count = plan.peers - 1 if plan.split else 1
    parts = refs[:part_count]
    out_ref, kv_s, q_s, acc_s, carry_s, kv_sems, q_sems = refs[part_count:]
    me = me_ref[0]
    t = plan.member(me)
    w = plan.peer(me)
    copies = []
    number = 0
    for h in range(local_heads):
        for r in range(team):
            copies.append(
                pltpu.make_async_copy(
                    own_ref.at[r, h, pl.ds(0, rows), pl.ds(KV_LANES, ALL_LANES - KV_LANES)],
                    q_s.at[h, jnp.bitwise_xor(t, r)],
                    q_sems.at[h * team + r],
                )
            )
        if plan.split:
            for rw in range(plan.peers):
                for r in range(team):
                    source = own_ref if rw == 0 else parts[rw - 1]
                    position = jnp.bitwise_xor(me, plan.index(r, rw))
                    copies.append(
                        pltpu.make_async_copy(
                            source.at[r, h, :, pl.ds(0, KV_LANES)],
                            kv_s.at[h, position],
                            kv_sems.at[number],
                        )
                    )
                    number += 1
        else:
            copies.append(
                pltpu.make_async_copy(parts[0].at[:, h], kv_s.at[h], kv_sems.at[number])
            )
            number += 1
    for copy in copies:
        copy.start()
    acc_s[...] = jnp.zeros_like(acc_s)
    carry_s[...] = jnp.zeros_like(carry_s)
    for copy in copies:
        copy.wait()

    pair = 2 if plan.sp % 2 == 0 else 1
    span = pair * rows
    tri = (
        lax.broadcasted_iota(jnp.int32, (span, span), 0)
        > lax.broadcasted_iota(jnp.int32, (span, span), 1)
    ).astype(F32).astype(BF)
    scales = (BROAD_SIZE ** (-0.5), NARROW_SIZE ** (-0.5))
    group = 2 if team % 2 == 0 else 1
    for first in reversed(range(0, team, group)):
        count = group * rows
        places = [plan.index(k, w) for k in range(first, first + group)]
        query_positions = jnp.concatenate(
            [p * rows + lax.broadcasted_iota(jnp.int32, (rows, span), 0) for p in places], axis=0
        )
        gap = lax.broadcasted_iota(jnp.int32, (count, span), 1) - query_positions
        steps = places[-1] // pair + 1

        def body(step, _, first=first, count=count, gap=gap, steps=steps):
            chunk = steps - 1 - step
            causal = gap < -chunk * span
            for h in range(local_heads):
                tails = [
                    kv_s[h, chunk * pair + b, pl.ds(rows, EXTRA), :].astype(F32)
                    for b in range(pair)
                ]
                tails = [a[:, :rows] + a[:, rows : 2 * rows] + a[:, 2 * rows : 3 * rows] for a in tails]
                offsets = jnp.concatenate(tails, axis=1)
                lanes = kv_s[h, pl.ds(chunk * pair, pair), pl.ds(0, rows), :]
                for g in range(2):
                    keys = lanes[:, :, 2 * LANES * g : 2 * LANES * g + LANES].reshape(span, LANES)
                    values = keys if g else lanes[:, :, LANES : 2 * LANES].reshape(span, LANES)
                    queries = q_s[h, first : first + group, :, g * LANES : (g + 1) * LANES]
                    queries = queries.reshape(count, LANES)
                    logits = lax.dot_general(
                        queries, keys, (((1,), (1,)), ((), ())), preferred_element_type=F32
                    )
                    logits = logits * scales[g] + offsets[g : g + 1]
                    logits = jnp.where(causal, logits, NEG)
                    lognot = jnp.minimum(-logits, 0.0) - jnp.log(1.0 + jnp.exp(-jnp.abs(logits)))
                    later = jnp.dot(lognot.astype(BF), tri, preferred_element_type=F32)
                    here = pl.ds(first * rows, count)
                    carry = carry_s[h, g, here, :]
                    wide = jnp.concatenate([carry] * (span // LANES), axis=1)
                    weights = jnp.exp(logits + lognot + (later + wide)).astype(BF)
                    acc_s[h, g, here, :] += jnp.dot(weights, values, preferred_element_type=F32)
                    carry_s[h, g, here, :] = carry + (later[:, :1] + lognot[:, :1])
            return 0

        lax.fori_loop(0, steps, body, 0)
    for h in range(local_heads):
        for g in range(2):
            out_ref[h, :, g * LANES : (g + 1) * LANES] = acc_s[h, g].astype(BF)


def attention(plan, me, own, parts):
    team, local_heads, tall, _ = own.shape
    rows = tall - EXTRA
    total = team * rows
    pieces = plan.sp if plan.split else 1
    work = local_heads * 2 * total * plan.sp * rows
    return pl.pallas_call(
        functools.partial(attention_kernel, plan),
        out_shape=jax.ShapeDtypeStruct((local_heads, total, 2 * LANES), BF),
        in_specs=[SMEM, ANY] + [ANY] * len(parts),
        out_specs=VMEM,
        scratch_shapes=[
            pltpu.VMEM((local_heads, plan.sp, tall, KV_LANES), BF),
            pltpu.VMEM((local_heads, team, rows, 2 * LANES), BF),
            pltpu.VMEM((local_heads, 2, total, LANES), F32),
            pltpu.VMEM((local_heads, 2, total, LANES), F32),
            pltpu.SemaphoreType.DMA((local_heads * pieces,)),
            pltpu.SemaphoreType.DMA((local_heads * team,)),
        ],
        cost_estimate=cost(work * 4 * LANES, 8 * own.size, 3 * work),
        name="attention",
    )(me, own, *parts)


def project_kernel(plan, me_ref, broad_ref, narrow_ref, *refs):
    team = plan.team
    attended = refs[:team]
    out_ref, a_s, w_s = refs[team:]
    local_heads, total, _ = attended[0].shape
    t = plan.member(me_ref[0])
    depth = out_ref.shape[1]
    for r in range(team):
        for h in range(local_heads):
            at = (r * local_heads + h) * 2 * LANES
            head = jnp.bitwise_xor(t, r) * local_heads + h
            a_s[:, pl.ds(at, 2 * LANES)] = attended[r][h]
            w_s[pl.ds(at, LANES), :] = broad_ref[
                pl.ds(pl.multiple_of(head * BROAD_SIZE, BROAD_SIZE), BROAD_SIZE), :
            ]
            w_s[pl.ds(at + LANES, NARROW_SIZE), :] = jnp.zeros((NARROW_SIZE, depth), BF)
            w_s[pl.ds(at + LANES + NARROW_SIZE, NARROW_SIZE), :] = narrow_ref[
                pl.ds(pl.multiple_of(head * NARROW_SIZE, NARROW_SIZE), NARROW_SIZE), :
            ]
    width = min(512, depth)
    for n in range(0, depth, width):
        out_ref[:, pl.ds(n, width)] = jnp.dot(
            a_s[...], w_s[:, pl.ds(n, width)], preferred_element_type=F32
        ).astype(BF)


def project(plan, me, attended, out_broad, out_narrow):
    local_heads, total, _ = attended[0].shape
    depth = out_broad.shape[1]
    inner = plan.team * local_heads * 2 * LANES
    return pl.pallas_call(
        functools.partial(project_kernel, plan),
        out_shape=jax.ShapeDtypeStruct((total, depth), BF),
        in_specs=[SMEM] + [VMEM] * (2 + len(attended)),
        out_specs=VMEM,
        scratch_shapes=[pltpu.VMEM((total, inner), BF), pltpu.VMEM((inner, depth), BF)],
        cost_estimate=cost(2 * total * inner * depth, 2 * total * depth),
        name="project",
    )(me, out_broad, out_narrow, *attended)


def mixer_kernel(plan, gate_parts, down_parts, me_ref, gain_ref, mine_ref, other_ref, *refs):
    team, tp = plan.team, plan.tp
    streams = refs[:team]
    refs = refs[team:]
    gates, refs = refs[:gate_parts], refs[gate_parts:]
    downs, refs = refs[:down_parts], refs[down_parts:]
    mid_ref, mixed_ref, gu_s, down_s, normed_s, mid_s, gu_sems, down_sems = refs
    me, core = me_ref[0], me_ref[1]
    t = plan.member(me)
    rows, depth = streams[0].shape
    band = gu_s.shape[0] // plan.sp
    units = down_s.shape[0]
    column = depth // plan.sp
    gate_copies, down_copies = [], []
    if plan.split:
        for rw in range(plan.peers):
            for r in range(team):
                place = jnp.bitwise_xor(me, plan.index(r, rw))
                number = rw * team + r
                gate_copies.append(
                    pltpu.make_async_copy(
                        gates[rw].at[r],
                        gu_s.at[pl.ds(pl.multiple_of(place * band, band), band), :],
                        gu_sems.at[number],
                    )
                )
                down_copies.append(
                    pltpu.make_async_copy(
                        downs[rw].at[r],
                        down_s.at[:, pl.ds(pl.multiple_of(place * column, column), column)],
                        down_sems.at[number],
                    )
                )
    else:
        gate_copies.append(pltpu.make_async_copy(gates[0], gu_s, gu_sems.at[0]))
        down_copies.append(pltpu.make_async_copy(downs[0], down_s, down_sems.at[0]))
    for copy in gate_copies + down_copies:
        copy.start()
    for r in range(team):
        at = pl.ds(pl.multiple_of(jnp.bitwise_xor(t, r) * rows, rows), rows)
        mid = (
            streams[r][...].astype(F32)
            + (mine_ref[at, :].astype(F32) + other_ref[at, :].astype(F32))
        ).astype(BF)
        if r == 0:
            mid_s[...] = mid
        middle = mid.astype(F32)
        scaled = middle * lax.rsqrt(jnp.mean(middle * middle, axis=1, keepdims=True) + norm_eps)
        normed_s[at, :] = (scaled * gain_ref[...]).astype(BF)
    share = rows // tp
    mid_ref[...] = mid_s[pl.ds(pl.multiple_of(core * share, share), share), :]
    for copy in gate_copies:
        copy.wait()
    gate = jnp.dot(normed_s[...], gu_s[:, :units], preferred_element_type=F32)
    up = jnp.dot(normed_s[...], gu_s[:, units:], preferred_element_type=F32)
    hidden = (gate / (1.0 + jnp.exp(-gate)) * up).astype(BF)
    for copy in down_copies:
        copy.wait()
    width = min(512, depth)
    for n in range(0, depth, width):
        part = jnp.dot(hidden, down_s[:, pl.ds(n, width)], preferred_element_type=F32).astype(BF)
        for c in range(tp):
            for k in range(team):
                mixed_ref[c, k, :, pl.ds(n, width)] = part[
                    k * rows + c * share : k * rows + (c + 1) * share
                ]


def mixer(plan, place, gain, mine, other, streams, gates, downs):
    rows, depth = streams[0].shape
    total = plan.team * rows
    units = downs[0].shape[-2]
    share = rows // plan.tp
    pieces = plan.sp if plan.split else 1
    return pl.pallas_call(
        functools.partial(mixer_kernel, plan, len(gates), len(downs)),
        out_shape=(
            jax.ShapeDtypeStruct((share, depth), BF),
            jax.ShapeDtypeStruct((plan.tp, plan.team, share, depth), BF),
        ),
        in_specs=[SMEM] + [VMEM] * (3 + plan.team) + [ANY] * (len(gates) + len(downs)),
        out_specs=(VMEM, VMEM),
        scratch_shapes=[
            pltpu.VMEM((depth, 2 * units), BF),
            pltpu.VMEM((units, depth), BF),
            pltpu.VMEM((total, depth), BF),
            pltpu.VMEM((rows, depth), BF),
            pltpu.SemaphoreType.DMA((pieces,)),
            pltpu.SemaphoreType.DMA((pieces,)),
        ],
        cost_estimate=cost(6 * total * depth * units, 8 * total * depth),
        name="mixer",
    )(place, gain, mine, other, *streams, *gates, *downs)


def by_head(array, heads):
    rows = array.shape[0]
    return jnp.transpose(array.reshape(rows, heads, -1), (1, 0, 2))


def local(
    plan,
    stream,
    query_narrow,
    query_broad,
    key_narrow,
    key_broad,
    value_narrow,
    value_broad,
    key_offsets,
    out_narrow,
    out_broad,
    norm_gain,
    gate_weight,
    up_weight,
    down_weight,
):
    team, peers, tp = plan.team, plan.peers, plan.tp
    rows, depth = stream.shape
    heads = query_narrow.shape[1] // NARROW_SIZE
    i = lax.axis_index("sp").astype(jnp.int32)
    core = lax.axis_index("tp").astype(jnp.int32)
    t = plan.member(i)
    place = jnp.stack([i, core])

    narrow = functools.partial(by_head, heads=heads)
    body = jnp.concatenate(
        [
            narrow(key_broad),
            narrow(value_broad),
            narrow(key_narrow),
            narrow(value_narrow),
            narrow(query_broad),
            narrow(query_narrow),
            jnp.zeros((heads, rows, NARROW_SIZE), BF),
        ],
        axis=2,
    )
    high = lax.reduce_precision(key_offsets, 8, 7)
    middle = lax.reduce_precision(key_offsets - high, 8, 7)
    low = key_offsets - high - middle
    pieces = jnp.stack([high, middle, low]).astype(BF).reshape(3, rows, heads, 2)
    pieces = jnp.transpose(pieces, (2, 3, 0, 1))[:, ::-1].reshape(heads, 2, 3 * rows)
    tail = jnp.pad(pieces, ((0, 0), (0, EXTRA - 2), (0, ALL_LANES - 3 * rows)))
    packed = jnp.concatenate([body, tail], axis=1)
    packed = packed.reshape(team, heads // team, rows + EXTRA, ALL_LANES)

    units = gate_weight.shape[1] // team
    joined = jnp.concatenate(
        [
            jnp.transpose(gate_weight.reshape(-1, team, units), (1, 0, 2)),
            jnp.transpose(up_weight.reshape(-1, team, units), (1, 0, 2)),
        ],
        axis=2,
    )
    downs = down_weight.reshape(team, units, -1)

    if plan.split:
        own = [pick(packed, t)]
        own += [plan.team_swap(pick(packed, t ^ r), r) for r in range(1, team)]
        own = jnp.stack(own)
        keys = own[..., :KV_LANES]
        parts = [plan.peer_swap(keys, r) for r in range(1, peers)]
        streams = [stream] + [plan.team_swap(stream, r) for r in range(1, team)]
        gate_own = jnp.stack(
            [pick(joined, t)] + [plan.team_swap(pick(joined, t ^ r), r) for r in range(1, team)]
        )
        down_own = jnp.stack(
            [pick(downs, t)] + [plan.team_swap(pick(downs, t ^ r), r) for r in range(1, team)]
        )
        gates = [gate_own] + [plan.peer_swap(gate_own, r) for r in range(1, peers)]
        down_parts = [down_own] + [plan.peer_swap(down_own, r) for r in range(1, peers)]
    else:
        own = packed
        keys = own[0, :, :, :KV_LANES]
        parts = [lax.all_gather(keys, "sp", axis=0)]
        streams = [stream]
        gates = [lax.all_gather(joined[0], "sp", axis=0, tiled=True)]
        down_parts = [lax.all_gather(downs[0], "sp", axis=1, tiled=True)]

    mine = attention(plan, place, own, parts)
    attended = [mine] + [plan.team_swap(mine, r) for r in range(1, team)]
    partial = project(plan, place, attended, out_broad, out_narrow)
    if tp == 2:
        other = lax.ppermute(partial, "tp", [(0, 1), (1, 0)])
    else:
        summed = lax.psum(partial.astype(F32), "tp")
        partial, other = summed.astype(BF), jnp.zeros_like(partial)
    mid, mixed = mixer(
        plan, place, norm_gain.reshape(1, depth), partial, other, streams, gates, down_parts
    )
    sums = pick(mixed, core).astype(F32)
    if tp & (tp - 1) == 0:
        for c in range(1, tp):
            sent = lax.ppermute(pick(mixed, core ^ c), "tp", [(j, j ^ c) for j in range(tp)])
            sums = sums + sent.astype(F32)
    else:
        sums = lax.psum_scatter(mixed, "tp", scatter_dimension=0).astype(F32)
    sums = sums.astype(BF)
    result = mid.astype(F32) + pick(sums, t).astype(F32)
    for r in range(1, team):
        result = result + plan.team_swap(pick(sums, t ^ r), r).astype(F32)
    return result.astype(BF)


def solution(mesh):
    split = P("sp", "tp")
    placed = (P("sp", None),) + (split,) * 7 + (P("tp", None),) * 2 + (P(),)
    placed = placed + (split, split, P("tp", "sp"))
    sizes = dict(mesh.shape)

    def whole(*arrays):
        heads = arrays[1].shape[1] // NARROW_SIZE // sizes["tp"]
        hidden = arrays[11].shape[1] // sizes["tp"]
        plan = Plan(sizes["sp"], sizes["tp"], heads, hidden)
        return jax.shard_map(
            functools.partial(local, plan),
            mesh=mesh,
            in_specs=placed,
            out_specs=P(("sp", "tp"), None),
            check_vma=False,
        )(*arrays)

    return whole
```

time: 1460 us -> 267 us (0.18)
  other arithmetic: 798 us -> 5.15 us
  waiting for transfers between devices: 461 us -> 185 us
  matrix products: 67.9 us -> 0 us
  local copies, waits for them, and re-layouts: 53.3 us -> 13.2 us
  blocking collectives: 34.9 us -> 0 us
  starting transfers between devices: 0.33 us -> 32.4 us
  Pallas kernels: 0 us -> 30.5 us
  loops' own time: 20 us -> 0 us
    another operation x14 -> x5, other arithmetic: 780 us -> 2.5 us  [the longest x1 0.99 us: local(): jnp.stack([pick(downs, t)] + [plan.team_swap(pick(downs, t ^ r), r) for r...]
    all_gather x7 -> x0, waiting for transfers between devices: 445 us -> none  [the longest x1 116 us: local(): down_full = lax.all_gather(down_weight, 'sp', axis=1, tiled=True)]
    ppermute x0 -> x29, waiting for transfers between devices: none -> 185 us  [the longest x27 182 us: swap(): return lax.ppermute(array, 'sp', [(i, i ^ offset) for i in range(self.sp)])]
    dot_general x28 -> x0, matrix products: 67.9 us -> none  [the longest x8 31.9 us: weighted_values(): jnp.einsum('hqk,khd->qhd', weights, values, preferred_element_type=jnp.fl...]
    all_gather x2 -> x0, blocking collectives: 34.9 us -> none  [the longest x1 32.7 us: local(): lax.all_gather(key_offsets.astype(jnp.bfloat16), 'sp', axis=0, tiled=True)]
    dynamic_slice x28 -> x2, local copies, waits for them, and re-layouts: 35 us -> 0.81 us  [pick(): return lax.dynamic_index_in_dim(array, index, 0, keepdims=False)]
    ppermute x0 -> x29, starting transfers between devices: none -> 32.4 us  [the longest x27 32.3 us: swap(): return lax.ppermute(array, 'sp', [(i, i ^ offset) for i in range(self.sp)])]
    pallas_call x0 -> x3, Pallas kernels: none -> 30.5 us  [the longest x1 13.1 us: attention(): pl.pallas_call(functools.partial(attention_kernel, plan), out_shape=jax.S...]
  transfers between devices with their start and end apart: 9 -> 29, of which waited for: 9 -> 20; matrix products, arithmetic and copies ran while one was open for 4% -> 1% of each run, Pallas kernels for 0% -> 0%
where the time goes in v1:
time: 267 us
  waiting for transfers between devices  185 us (69%)
  starting transfers between devices  32.4 us (12%)
  Pallas kernels  30.5 us (11%)
  local copies, waits for them, and re-layouts  13.2 us (5%)
  other arithmetic  5.15 us (2%)
    ppermute x27, waiting for transfers between devices, swap(): return lax.ppermute(array, 'sp', [(i, i ^ offset) for i in range(self.sp)])  182 us
    ppermute x27, starting transfers between devices, swap(): return lax.ppermute(array, 'sp', [(i, i ^ offset) for i in range(self.sp)])  32.3 us
    pallas_call x1, Pallas kernels, attention(): pl.pallas_call(functools.partial(attention_kernel, plan), out_shape=jax.S...  13.1 us
    pallas_call x1, Pallas kernels, mixer(): pl.pallas_call(functools.partial(mixer_kernel, plan, len(gates), len(down...  11.6 us
    unnamed x46, local copies, waits for them, and re-layouts  9.13 us
    pallas_call x1, Pallas kernels, project(): pl.pallas_call(functools.partial(project_kernel, plan), out_shape=jax.Sha...  5.82 us
  transfers between devices with their start and end apart: 29, of which 20 were waited for; matrix products, arithmetic and copies ran while one was open for 1% of the time, Pallas kernels for 0%

profile of v1, /device:TPU:24, one launch (start us, length us, event | category | flops | bytes accessed | tf_op | source)
XLA Modules:
  0.0 266.7 jit_solution(6681812829391489148)
XLA Ops:
  11.0 2.9 %collective-permute-done = bf16[1,136,640]{2,1,0:T(8,128)(2,1)S(1)} collective-permute-done((bf16[1,136,640]{2,1,0:T(8,128)(2,1)S(1)}, bf16[1,136,640]{2,1,0:T(8,128)(2,1)S(1)}, u32[]{:S(2)}, u32[]{:S(2)}) %collective-permute-start) | collective-permute-done | bytes 174112 | tf_op jit(solution)/shard_map/ppermute | solution.py:60
  13.9 2.4 collective-permute-done.1
  16.3 2.3 collective-permute-done.2
  18.7 1.6 collective-permute-start.3
  20.7 2.5 collective-permute-start.5
  23.8 5.3 %collective-permute-done.3.refs_0_ = bf16[4,1,136,384]{3,2,1,0:T(8,128)(2,1)S(1)} collective-permute-done((bf16[4,1,136,384]{3,2,1,0:T(8,128)(2,1)S(1)}, bf16[4,1,136,384]{3,2,1,0:T(8,128)(2,1)S(1)}, u32[]{:S(2)}, u32[]{:S(2)}) %collective-permute-start.3) | collective-permute-done | bytes 417824 | tf_op jit(solution)/shard_map/ppermute | solution.py:60
  29.0 20.0 %collective-permute-done.4.refs_1_ = bf16[4,1,136,384]{3,2,1,0:T(8,128)(2,1)S(1)} collective-permute-done((bf16[4,1,136,384]{3,2,1,0:T(8,128)(2,1)S(1)}, bf16[4,1,136,384]{3,2,1,0:T(8,128)(2,1)S(1)}, u32[]{:S(2)}, u32[]{:S(2)}) %collective-permute-start.4) | collective-permute-done | bytes 417824 | tf_op jit(solution)/shard_map/ppermute | solution.py:60
  49.1 8.8 %collective-permute-done.5.refs_2_ = bf16[4,1,136,384]{3,2,1,0:T(8,128)(2,1)S(1)} collective-permute-done((bf16[4,1,136,384]{3,2,1,0:T(8,128)(2,1)S(1)}, bf16[4,1,136,384]{3,2,1,0:T(8,128)(2,1)S(1)}, u32[]{:S(2)}, u32[]{:S(2)}) %collective-permute-start.5) | collective-permute-done | bytes 417824 | tf_op jit(solution)/shard_map/ppermute | solution.py:60
  58.6 13.1 %attention.1.refs_0_ = bf16[1,512,256]{2,1,0:T(8,128)(2,1)} custom-call(s32[2]{0:T(128)} %pad_add_fusion.me_ref, bf16[4,1,136,640]{3,2,1,0:T(8,128)(2,1)} %copy-done.3, bf16[4,1,136,384]{3,2,1,0:T(8,128)(2,1)} %copy-done.13, bf16[4,1,136,384]{3,2,1,0:T(8,128)(2,1)} %copy-done.14, bf16[4,1,136,384]{3,2,1,0:T(8,128)(2,1)} %copy-done.15), custom_call_target="tpu_custom_call" | custom-call | flops 1073741824 | bytes 2785280 | tf_op jit(solution)/shard_map/attention/pallas_call | solution.py:184
  71.8 1.6 collective-permute-start.6
  73.3 2.0 collective-permute-start.8
  75.3 5.0 %collective-permute-done.6.refs_1_ = bf16[1,512,256]{2,1,0:T(8,128)(2,1)S(1)} collective-permute-done((bf16[1,512,256]{2,1,0:T(8,128)(2,1)}, bf16[1,512,256]{2,1,0:T(8,128)(2,1)S(1)}, u32[]{:S(2)}, u32[]{:S(2)}) %collective-permute-start.6) | collective-permute-done | bytes 262176 | tf_op jit(solution)/shard_map/ppermute | solution.py:60
  80.3 2.4 collective-permute-done.7.refs_2_
  82.7 4.4 %collective-permute-done.8.refs_3_ = bf16[1,512,256]{2,1,0:T(8,128)(2,1)S(1)} collective-permute-done((bf16[1,512,256]{2,1,0:T(8,128)(2,1)}, bf16[1,512,256]{2,1,0:T(8,128)(2,1)S(1)}, u32[]{:S(2)}, u32[]{:S(2)}) %collective-permute-start.8) | collective-permute-done | bytes 262176 | tf_op jit(solution)/shard_map/ppermute | solution.py:60
  87.8 5.8 %project.1.mine_ref = bf16[512,2048]{1,0:T(8,128)(2,1)} custom-call(s32[2]{0:T(128)} %pad_add_fusion.me_ref, bf16[512,2048]{1,0:T(8,128)(2,1)} %broad_ref.1, bf16[256,2048]{1,0:T(8,128)(2,1)} %narrow_ref.1, bf16[1,512,256]{2,1,0:T(8,128)(2,1)} %attention.1.refs_0_, bf16[1,512,256]{2,1,0:T(8,128)(2,1)} %copy-done.16, bf16[1,512,256]{2,1,0:T(8,128)(2,1)} %copy-done.17, ...), custom_call_target="tpu_custom_call" | custom-call | flops 2147483648 | bytes 2097152 | tf_op jit(solution)/shard_map/project/pallas_call | solution.py:232
  96.1 1.7 collective-permute-start.21
  98.8 1.6 collective-permute-start.13
  104.2 3.2 %collective-permute-start.22 = (bf16[4,384,128]{2,1,0:T(8,128)(2,1)S(1)}, bf16[4,384,128]{2,1,0:T(8,128)(2,1)S(1)}, u32[]{:S(2)}, u32[]{:S(2)}) collective-permute-start(bf16[4,384,128]{2,1,0:T(8,128)(2,1)S(1)} %pad_maximum_fusion.2.refs_8_), channel_id=1, source_target_pairs={{0,4},{2,6},{4,0},{6,2},{8,12},{10,14},{12,8},{14,10},{16,20},{18,... | collective-permute-start | bytes 1179656 | tf_op jit(solution)/shard_map/ppermute | solution.py:60
  108.0 2.4 collective-permute-start.15
  110.9 4.3 %collective-permute-done.14 = bf16[128,768]{1,0:T(8,128)(2,1)S(1)} collective-permute-done((bf16[128,768]{1,0:T(8,128)(2,1)S(1)}, bf16[128,768]{1,0:T(8,128)(2,1)S(1)}, u32[]{:S(2)}, u32[]{:S(2)}) %collective-permute-start.14) | collective-permute-done | bytes 196640 | tf_op jit(solution)/shard_map/ppermute | solution.py:60
  115.3 3.2 %collective-permute-done.15 = bf16[128,768]{1,0:T(8,128)(2,1)S(1)} collective-permute-done((bf16[128,768]{1,0:T(8,128)(2,1)S(1)}, bf16[128,768]{1,0:T(8,128)(2,1)S(1)}, u32[]{:S(2)}, u32[]{:S(2)}) %collective-permute-start.15) | collective-permute-done | bytes 196640 | tf_op jit(solution)/shard_map/ppermute | solution.py:60
  118.5 2.2 collective-permute-start.11
  120.9 19.9 %collective-permute-done.23.refs_10_ = bf16[4,384,128]{2,1,0:T(8,128)(2,1)S(1)} collective-permute-done((bf16[4,384,128]{2,1,0:T(8,128)(2,1)S(1)}, bf16[4,384,128]{2,1,0:T(8,128)(2,1)S(1)}, u32[]{:S(2)}, u32[]{:S(2)}) %collective-permute-start.23) | collective-permute-done | bytes 393248 | tf_op jit(solution)/shard_map/ppermute | solution.py:60
  140.8 41.1 %collective-permute-done.24.refs_11_ = bf16[4,384,128]{2,1,0:T(8,128)(2,1)S(1)} collective-permute-done((bf16[4,384,128]{2,1,0:T(8,128)(2,1)S(1)}, bf16[4,384,128]{2,1,0:T(8,128)(2,1)S(1)}, u32[]{:S(2)}, u32[]{:S(2)}) %collective-permute-start.24) | collective-permute-done | bytes 393248 | tf_op jit(solution)/shard_map/ppermute | solution.py:60
  182.7 3.1 %collective-permute-start.18 = (bf16[4,128,768]{2,1,0:T(8,128)(2,1)S(1)}, bf16[4,128,768]{2,1,0:T(8,128)(2,1)}, u32[]{:S(2)}, u32[]{:S(2)}) collective-permute-start(bf16[4,128,768]{2,1,0:T(8,128)(2,1)S(1)} %pad_maximum_fusion.refs_4_), channel_id=1, source_target_pairs={{0,20},{2,22},{4,16},{6,18},{8,28},{10,30},{12,24},{14,26},{16,4},... | collective-permute-start | bytes 2359304 | tf_op jit(solution)/shard_map/ppermute | solution.py:60
  185.9 45.8 %collective-permute-done.12.refs_3_ = bf16[128,2048]{1,0:T(8,128)(2,1)} collective-permute-done((bf16[128,2048]{1,0:T(8,128)(2,1)}, bf16[128,2048]{1,0:T(8,128)(2,1)}, u32[]{:S(2)}, u32[]{:S(2)}) %collective-permute-start.12) | collective-permute-done | bytes 524320 | tf_op jit(solution)/shard_map/ppermute | solution.py:60
  233.0 11.6 %mixer.1 = (bf16[64,2048]{1,0:T(8,128)(2,1)}, bf16[2,4,64,2048]{3,2,1,0:T(8,128)(2,1)}) custom-call(s32[2]{0:T(128)} %pad_add_fusion.me_ref, f32[1,2048]{1,0:T(1,128)} %bitcast.86, bf16[512,2048]{1,0:T(8,128)(2,1)} %project.1.mine_ref, bf16[512,2048]{1,0:T(8,128)(2,1)} %copy-done.1, bf16[128,2048]{1,0:T(8,128)(2,1)} %refs_0_.1, ...), custom_call_target="tpu_custom_call" | custom-call | flops 2415919104 | bytes 8388608 | tf_op jit(solution)/shard_map/mixer/pallas_call | solution.py:317
  246.2 2.8 %collective-permute-done.25 = bf16[4,64,2048]{2,1,0:T(8,128)(2,1)} collective-permute-done((bf16[4,64,2048]{2,1,0:T(8,128)(2,1)S(1)}, bf16[4,64,2048]{2,1,0:T(8,128)(2,1)}, u32[]{:S(2)}, u32[]{:S(2)}) %collective-permute-start.25) | collective-permute-done | bytes 1048608 | tf_op jit(solution)/shard_map/ppermute | solution.py:437
  248.9 1.6 fusion
  250.8 3.4 %collective-permute-start.28 = (bf16[64,2048]{1,0:T(8,128)(2,1)S(1)}, bf16[64,2048]{1,0:T(8,128)(2,1)S(1)}, u32[]{:S(2)}, u32[]{:S(2)}) collective-permute-start(bf16[64,2048]{1,0:T(8,128)(2,1)S(1)} %get-tuple-element.10), channel_id=1, source_target_pairs={{0,10},{2,8},{4,14},{6,12},{8,2},{10,0},{12,6},{14,4},{16,26},{18,... | collective-permute-start | bytes 786440 | tf_op jit(solution)/shard_map/ppermute | solution.py:60
  254.2 4.9 %collective-permute-done.26 = bf16[64,2048]{1,0:T(8,128)(2,1)S(1)} collective-permute-done((bf16[64,2048]{1,0:T(8,128)(2,1)S(1)}, bf16[64,2048]{1,0:T(8,128)(2,1)S(1)}, u32[]{:S(2)}, u32[]{:S(2)}) %collective-permute-start.26) | collective-permute-done | bytes 262176 | tf_op jit(solution)/shard_map/ppermute | solution.py:60
  260.0 5.9 %collective-permute-done.28 = bf16[64,2048]{1,0:T(8,128)(2,1)S(1)} collective-permute-done((bf16[64,2048]{1,0:T(8,128)(2,1)S(1)}, bf16[64,2048]{1,0:T(8,128)(2,1)S(1)}, u32[]{:S(2)}, u32[]{:S(2)}) %collective-permute-start.28) | collective-permute-done | bytes 262176 | tf_op jit(solution)/shard_map/ppermute | solution.py:60
  (105 shorter events, 27.7 us)
Async XLA Ops:
  7.4 6.4 %collective-permute-start = (bf16[1,136,640]{2,1,0:T(8,128)(2,1)S(1)}, bf16[1,136,640]{2,1,0:T(8,128)(2,1)S(1)}, u32[]{:S(2)}, u32[]{:S(2)}) collective-permute-start(bf16[1,136,640]{2,1,0:T(8,128)(2,1)S(1)} %get-tuple-element.19), channel_id=1, source_target_pairs={{0,2},{2,0},{4,6},{6,4},{8,10},{10,8},{12,14},{14,12},{16,18},{18,... | collective-permute-start | bytes 522248 | tf_op jit(solution)/shard_map/ppermute | solution.py:60
  9.0 7.3 %collective-permute-start.1 = (bf16[1,136,640]{2,1,0:T(8,128)(2,1)S(1)}, bf16[1,136,640]{2,1,0:T(8,128)(2,1)S(1)}, u32[]{:S(2)}, u32[]{:S(2)}) collective-permute-start(bf16[1,136,640]{2,1,0:T(8,128)(2,1)S(1)} %get-tuple-element.18), channel_id=1, source_target_pairs={{0,8},{2,10},{4,12},{6,14},{8,0},{10,2},{12,4},{14,6},{16,24},{18,... | collective-permute-start | bytes 522248 | tf_op jit(solution)/shard_map/ppermute | solution.py:60
  9.4 9.1 %collective-permute-start.2 = (bf16[1,136,640]{2,1,0:T(8,128)(2,1)S(1)}, bf16[1,136,640]{2,1,0:T(8,128)(2,1)S(1)}, u32[]{:S(2)}, u32[]{:S(2)}) collective-permute-start(bf16[1,136,640]{2,1,0:T(8,128)(2,1)S(1)} %get-tuple-element.17), channel_id=1, source_target_pairs={{0,10},{2,8},{4,14},{6,12},{8,2},{10,0},{12,6},{14,4},{16,26},{18,... | collective-permute-start | bytes 522248 | tf_op jit(solution)/shard_map/ppermute | solution.py:60
  18.7 10.3 %collective-permute-start.3 = (bf16[4,1,136,384]{3,2,1,0:T(8,128)(2,1)S(1)}, bf16[4,1,136,384]{3,2,1,0:T(8,128)(2,1)S(1)}, u32[]{:S(2)}, u32[]{:S(2)}) collective-permute-start(bf16[4,1,136,384]{3,2,1,0:T(8,128)(2,1)S(1)} %slice.4), channel_id=1, source_target_pairs={{0,4},{2,6},{4,0},{6,2},{8,12},{10,14},{12,8},{14,10},{16,20},{18,... | collective-permute-start | bytes 1253384 | tf_op jit(solution)/shard_map/ppermute | solution.py:60
  20.3 28.8 %collective-permute-start.4 = (bf16[4,1,136,384]{3,2,1,0:T(8,128)(2,1)S(1)}, bf16[4,1,136,384]{3,2,1,0:T(8,128)(2,1)S(1)}, u32[]{:S(2)}, u32[]{:S(2)}) collective-permute-start(bf16[4,1,136,384]{3,2,1,0:T(8,128)(2,1)S(1)} %slice.4), channel_id=1, source_target_pairs={{0,16},{2,18},{4,20},{6,22},{8,24},{10,26},{12,28},{14,30},{16,0},... | collective-permute-start | bytes 1253384 | tf_op jit(solution)/shard_map/ppermute | solution.py:60
  20.7 37.2 %collective-permute-start.5 = (bf16[4,1,136,384]{3,2,1,0:T(8,128)(2,1)S(1)}, bf16[4,1,136,384]{3,2,1,0:T(8,128)(2,1)S(1)}, u32[]{:S(2)}, u32[]{:S(2)}) collective-permute-start(bf16[4,1,136,384]{3,2,1,0:T(8,128)(2,1)S(1)} %slice.4), channel_id=1, source_target_pairs={{0,20},{2,22},{4,16},{6,18},{8,28},{10,30},{12,24},{14,26},{16,4},... | collective-permute-start | bytes 1253384 | tf_op jit(solution)/shard_map/ppermute | solution.py:60
  71.8 8.5 %collective-permute-start.6 = (bf16[1,512,256]{2,1,0:T(8,128)(2,1)}, bf16[1,512,256]{2,1,0:T(8,128)(2,1)S(1)}, u32[]{:S(2)}, u32[]{:S(2)}) collective-permute-start(bf16[1,512,256]{2,1,0:T(8,128)(2,1)} %attention.1.refs_0_), channel_id=1, source_target_pairs={{0,2},{2,0},{4,6},{6,4},{8,10},{10,8},{12,14},{14,12},{16,18},{18,... | collective-permute-start | bytes 786440 | tf_op jit(solution)/shard_map/ppermute | solution.py:60
  73.3 9.4 %collective-permute-start.7 = (bf16[1,512,256]{2,1,0:T(8,128)(2,1)}, bf16[1,512,256]{2,1,0:T(8,128)(2,1)S(1)}, u32[]{:S(2)}, u32[]{:S(2)}) collective-permute-start(bf16[1,512,256]{2,1,0:T(8,128)(2,1)} %attention.1.refs_0_), channel_id=1, source_target_pairs={{0,8},{2,10},{4,12},{6,14},{8,0},{10,2},{12,4},{14,6},{16,24},{18,... | collective-permute-start | bytes 786440 | tf_op jit(solution)/shard_map/ppermute | solution.py:60
  73.3 13.7 %collective-permute-start.8 = (bf16[1,512,256]{2,1,0:T(8,128)(2,1)}, bf16[1,512,256]{2,1,0:T(8,128)(2,1)S(1)}, u32[]{:S(2)}, u32[]{:S(2)}) collective-permute-start(bf16[1,512,256]{2,1,0:T(8,128)(2,1)} %attention.1.refs_0_), channel_id=1, source_target_pairs={{0,10},{2,8},{4,14},{6,12},{8,2},{10,0},{12,6},{14,4},{16,26},{18,... | collective-permute-start | bytes 786440 | tf_op jit(solution)/shard_map/ppermute | solution.py:60
  93.6 138.1 %collective-permute-start.9 = (bf16[512,2048]{1,0:T(8,128)(2,1)}, bf16[512,2048]{1,0:T(8,128)(2,1)S(1)}, u32[]{:S(2)}, u32[]{:S(2)}) collective-permute-start(bf16[512,2048]{1,0:T(8,128)(2,1)} %project.1.mine_ref), channel_id=1, source_target_pairs={{0,1},{1,0},{2,3},{3,2},{4,5},{5,4},{6,7},{7,6},{8,9},{9,8},{10,11... | collective-permute-start | bytes 6291464 | tf_op jit(solution)/shard_map/ppermute | solution.py:427
  94.3 6.1 %collective-permute-start.19 = (bf16[384,128]{1,0:T(8,128)(2,1)}, bf16[384,128]{1,0:T(8,128)(2,1)S(1)}, u32[]{:S(2)}, u32[]{:S(2)}) collective-permute-start(bf16[384,128]{1,0:T(8,128)(2,1)} %get-tuple-element.23), channel_id=1, source_target_pairs={{0,2},{2,0},{4,6},{6,4},{8,10},{10,8},{12,14},{14,12},{16,18},{18,... | collective-permute-start | bytes 294920 | tf_op jit(solution)/shard_map/ppermute | solution.py:60
  95.8 6.0 %collective-permute-start.20 = (bf16[384,128]{1,0:T(8,128)(2,1)}, bf16[384,128]{1,0:T(8,128)(2,1)}, u32[]{:S(2)}, u32[]{:S(2)}) collective-permute-start(bf16[384,128]{1,0:T(8,128)(2,1)} %get-tuple-element.22), channel_id=1, source_target_pairs={{0,8},{2,10},{4,12},{6,14},{8,0},{10,2},{12,4},{14,6},{16,24},{18,... | collective-permute-start | bytes 294920 | tf_op jit(solution)/shard_map/ppermute | solution.py:60
  96.1 7.1 %collective-permute-start.21 = (bf16[384,128]{1,0:T(8,128)(2,1)}, bf16[384,128]{1,0:T(8,128)(2,1)}, u32[]{:S(2)}, u32[]{:S(2)}) collective-permute-start(bf16[384,128]{1,0:T(8,128)(2,1)} %get-tuple-element.21), channel_id=1, source_target_pairs={{0,10},{2,8},{4,14},{6,12},{8,2},{10,0},{12,6},{14,4},{16,26},{18,... | collective-permute-start | bytes 294920 | tf_op jit(solution)/shard_map/ppermute | solution.py:60
  98.8 11.6 %collective-permute-start.13 = (bf16[128,768]{1,0:T(8,128)(2,1)S(1)}, bf16[128,768]{1,0:T(8,128)(2,1)S(1)}, u32[]{:S(2)}, u32[]{:S(2)}) collective-permute-start(bf16[128,768]{1,0:T(8,128)(2,1)S(1)} %get-tuple-element.13), channel_id=1, source_target_pairs={{0,2},{2,0},{4,6},{6,4},{8,10},{10,8},{12,14},{14,12},{16,18},{18,... | collective-permute-start | bytes 589832 | tf_op jit(solution)/shard_map/ppermute | solution.py:60
  104.2 127.5 %copy-start.4 = (bf16[4,384,128]{2,1,0:T(8,128)(2,1)}, bf16[4,384,128]{2,1,0:T(8,128)(2,1)S(1)}, u32[]{:S(2)}) copy-start(bf16[4,384,128]{2,1,0:T(8,128)(2,1)S(1)} %pad_maximum_fusion.2.refs_8_) | copy-start | bytes 1179652
  104.2 14.3 %collective-permute-start.22 = (bf16[4,384,128]{2,1,0:T(8,128)(2,1)S(1)}, bf16[4,384,128]{2,1,0:T(8,128)(2,1)S(1)}, u32[]{:S(2)}, u32[]{:S(2)}) collective-permute-start(bf16[4,384,128]{2,1,0:T(8,128)(2,1)S(1)} %pad_maximum_fusion.2.refs_8_), channel_id=1, source_target_pairs={{0,4},{2,6},{4,0},{6,2},{8,12},{10,14},{12,8},{14,10},{16,20},{18,... | collective-permute-start | bytes 1179656 | tf_op jit(solution)/shard_map/ppermute | solution.py:60
  107.4 7.8 %collective-permute-start.14 = (bf16[128,768]{1,0:T(8,128)(2,1)S(1)}, bf16[128,768]{1,0:T(8,128)(2,1)S(1)}, u32[]{:S(2)}, u32[]{:S(2)}) collective-permute-start(bf16[128,768]{1,0:T(8,128)(2,1)S(1)} %get-tuple-element.14), channel_id=1, source_target_pairs={{0,8},{2,10},{4,12},{6,14},{8,0},{10,2},{12,4},{14,6},{16,24},{18,... | collective-permute-start | bytes 589832 | tf_op jit(solution)/shard_map/ppermute | solution.py:60
  108.0 10.5 %collective-permute-start.15 = (bf16[128,768]{1,0:T(8,128)(2,1)S(1)}, bf16[128,768]{1,0:T(8,128)(2,1)S(1)}, u32[]{:S(2)}, u32[]{:S(2)}) collective-permute-start(bf16[128,768]{1,0:T(8,128)(2,1)S(1)} %get-tuple-element.15), channel_id=1, source_target_pairs={{0,10},{2,8},{4,14},{6,12},{8,2},{10,0},{12,6},{14,4},{16,26},{18,... | collective-permute-start | bytes 589832 | tf_op jit(solution)/shard_map/ppermute | solution.py:60
  110.4 71.6 %collective-permute-start.10 = (bf16[128,2048]{1,0:T(8,128)(2,1)}, bf16[128,2048]{1,0:T(8,128)(2,1)}, u32[]{:S(2)}, u32[]{:S(2)}) collective-permute-start(bf16[128,2048]{1,0:T(8,128)(2,1)} %refs_0_.1), channel_id=1, source_target_pairs={{0,2},{2,0},{4,6},{6,4},{8,10},{10,8},{12,14},{14,12},{16,18},{18,... | collective-permute-start | bytes 1572872 | tf_op jit(solution)/shard_map/ppermute | solution.py:60
  115.3 25.5 %collective-permute-start.23 = (bf16[4,384,128]{2,1,0:T(8,128)(2,1)S(1)}, bf16[4,384,128]{2,1,0:T(8,128)(2,1)S(1)}, u32[]{:S(2)}, u32[]{:S(2)}) collective-permute-start(bf16[4,384,128]{2,1,0:T(8,128)(2,1)S(1)} %pad_maximum_fusion.2.refs_8_), channel_id=1, source_target_pairs={{0,16},{2,18},{4,20},{6,22},{8,24},{10,26},{12,28},{14,30},{16,0},... | collective-permute-start | bytes 1179656 | tf_op jit(solution)/shard_map/ppermute | solution.py:60
  118.5 63.4 %collective-permute-start.24 = (bf16[4,384,128]{2,1,0:T(8,128)(2,1)S(1)}, bf16[4,384,128]{2,1,0:T(8,128)(2,1)S(1)}, u32[]{:S(2)}, u32[]{:S(2)}) collective-permute-start(bf16[4,384,128]{2,1,0:T(8,128)(2,1)S(1)} %pad_maximum_fusion.2.refs_8_), channel_id=1, source_target_pairs={{0,20},{2,22},{4,16},{6,18},{8,28},{10,30},{12,24},{14,26},{16,4},... | collective-permute-start | bytes 1179656 | tf_op jit(solution)/shard_map/ppermute | solution.py:60
  118.5 67.3 %collective-permute-start.11 = (bf16[128,2048]{1,0:T(8,128)(2,1)}, bf16[128,2048]{1,0:T(8,128)(2,1)}, u32[]{:S(2)}, u32[]{:S(2)}) collective-permute-start(bf16[128,2048]{1,0:T(8,128)(2,1)} %refs_0_.1), channel_id=1, source_target_pairs={{0,8},{2,10},{4,12},{6,14},{8,0},{10,2},{12,4},{14,6},{16,24},{18,... | collective-permute-start | bytes 1572872 | tf_op jit(solution)/shard_map/ppermute | solution.py:60
  120.9 110.8 %copy-start = (bf16[4,128,768]{2,1,0:T(8,128)(2,1)}, bf16[4,128,768]{2,1,0:T(8,128)(2,1)S(1)}, u32[]{:S(2)}) copy-start(bf16[4,128,768]{2,1,0:T(8,128)(2,1)S(1)} %pad_maximum_fusion.refs_4_) | copy-start | bytes 2359300
  140.7 41.2 %copy-start.6 = (bf16[4,384,128]{2,1,0:T(8,128)(2,1)}, bf16[4,384,128]{2,1,0:T(8,128)(2,1)S(1)}, u32[]{:S(2)}) copy-start(bf16[4,384,128]{2,1,0:T(8,128)(2,1)S(1)} %collective-permute-done.23.refs_10_) | copy-start | bytes 1179652
  140.7 90.9 %collective-permute-start.16 = (bf16[4,128,768]{2,1,0:T(8,128)(2,1)S(1)}, bf16[4,128,768]{2,1,0:T(8,128)(2,1)}, u32[]{:S(2)}, u32[]{:S(2)}) collective-permute-start(bf16[4,128,768]{2,1,0:T(8,128)(2,1)S(1)} %pad_maximum_fusion.refs_4_), channel_id=1, source_target_pairs={{0,4},{2,6},{4,0},{6,2},{8,12},{10,14},{12,8},{14,10},{16,20},{18,... | collective-permute-start | bytes 2359304 | tf_op jit(solution)/shard_map/ppermute | solution.py:60
  181.9 49.7 %collective-permute-start.17 = (bf16[4,128,768]{2,1,0:T(8,128)(2,1)S(1)}, bf16[4,128,768]{2,1,0:T(8,128)(2,1)}, u32[]{:S(2)}, u32[]{:S(2)}) collective-permute-start(bf16[4,128,768]{2,1,0:T(8,128)(2,1)S(1)} %pad_maximum_fusion.refs_4_), channel_id=1, source_target_pairs={{0,16},{2,18},{4,20},{6,22},{8,24},{10,26},{12,28},{14,30},{16,0},... | collective-permute-start | bytes 2359304 | tf_op jit(solution)/shard_map/ppermute | solution.py:60
  182.7 48.9 %collective-permute-start.18 = (bf16[4,128,768]{2,1,0:T(8,128)(2,1)S(1)}, bf16[4,128,768]{2,1,0:T(8,128)(2,1)}, u32[]{:S(2)}, u32[]{:S(2)}) collective-permute-start(bf16[4,128,768]{2,1,0:T(8,128)(2,1)S(1)} %pad_maximum_fusion.refs_4_), channel_id=1, source_target_pairs={{0,20},{2,22},{4,16},{6,18},{8,28},{10,30},{12,24},{14,26},{16,4},... | collective-permute-start | bytes 2359304 | tf_op jit(solution)/shard_map/ppermute | solution.py:60
  185.9 45.8 %collective-permute-start.12 = (bf16[128,2048]{1,0:T(8,128)(2,1)}, bf16[128,2048]{1,0:T(8,128)(2,1)}, u32[]{:S(2)}, u32[]{:S(2)}) collective-permute-start(bf16[128,2048]{1,0:T(8,128)(2,1)} %refs_0_.1), channel_id=1, source_target_pairs={{0,10},{2,8},{4,14},{6,12},{8,2},{10,0},{12,6},{14,4},{16,26},{18,... | collective-permute-start | bytes 1572872 | tf_op jit(solution)/shard_map/ppermute | solution.py:60
  246.1 2.9 %collective-permute-start.25 = (bf16[4,64,2048]{2,1,0:T(8,128)(2,1)S(1)}, bf16[4,64,2048]{2,1,0:T(8,128)(2,1)}, u32[]{:S(2)}, u32[]{:S(2)}) collective-permute-start(bf16[4,64,2048]{2,1,0:T(8,128)(2,1)S(1)} %dynamic-slice_bitcast_fusion), channel_id=1, source_target_pairs={{0,1},{1,0},{2,3},{3,2},{4,5},{5,4},{6,7},{7,6},{8,9},{9,8},{10,11... | collective-permute-start | bytes 3145736 | tf_op jit(solution)/shard_map/ppermute | solution.py:437
  250.6 8.4 %collective-permute-start.26 = (bf16[64,2048]{1,0:T(8,128)(2,1)S(1)}, bf16[64,2048]{1,0:T(8,128)(2,1)S(1)}, u32[]{:S(2)}, u32[]{:S(2)}) collective-permute-start(bf16[64,2048]{1,0:T(8,128)(2,1)S(1)} %get-tuple-element.9), channel_id=1, source_target_pairs={{0,2},{2,0},{4,6},{6,4},{8,10},{10,8},{12,14},{14,12},{16,18},{18,... | collective-permute-start | bytes 786440 | tf_op jit(solution)/shard_map/ppermute | solution.py:60
  250.7 9.2 %collective-permute-start.27 = (bf16[64,2048]{1,0:T(8,128)(2,1)S(1)}, bf16[64,2048]{1,0:T(8,128)(2,1)S(1)}, u32[]{:S(2)}, u32[]{:S(2)}) collective-permute-start(bf16[64,2048]{1,0:T(8,128)(2,1)S(1)} %get-tuple-element.11), channel_id=1, source_target_pairs={{0,8},{2,10},{4,12},{6,14},{8,0},{10,2},{12,4},{14,6},{16,24},{18,... | collective-permute-start | bytes 786440 | tf_op jit(solution)/shard_map/ppermute | solution.py:60
  250.8 15.0 %collective-permute-start.28 = (bf16[64,2048]{1,0:T(8,128)(2,1)S(1)}, bf16[64,2048]{1,0:T(8,128)(2,1)S(1)}, u32[]{:S(2)}, u32[]{:S(2)}) collective-permute-start(bf16[64,2048]{1,0:T(8,128)(2,1)S(1)} %get-tuple-element.10), channel_id=1, source_target_pairs={{0,10},{2,8},{4,14},{6,12},{8,2},{10,0},{12,6},{14,4},{16,26},{18,... | collective-permute-start | bytes 786440 | tf_op jit(solution)/shard_map/ppermute | solution.py:60
  (16 other events, 176.9 us)

commit v2 on v1

--- a/solution.py
+++ b/solution.py
@@ -1,5 +1,4 @@
 import functools
-import math
 
 import jax
 import jax.numpy as jnp
@@ -7,6 +6,7 @@
 from jax.experimental import pallas as pl
 from jax.experimental.pallas import tpu as pltpu
 from jax.sharding import PartitionSpec as P
+
 
 NARROW_SIZE = 64
 BROAD_SIZE = 128
@@ -22,14 +22,15 @@
 VMEM = pl.BlockSpec(memory_space=pltpu.VMEM)
 SMEM = pl.BlockSpec(memory_space=pltpu.SMEM)
 
-TEAM_BITS = (0, 2)
-PEER_BITS = (1, 3)
+TEAM_BITS = (2, 3)
+PEER_BITS = (0, 1)
 
 
 class Plan:
-    def __init__(self, sp, tp, heads, hidden):
+    def __init__(self, sp, tp, heads, hidden, depth):
         self.sp, self.tp = sp, tp
-        self.split = sp == 16 and heads % 4 == 0 and hidden % (4 * LANES) == 0
+        self.split = sp == 16 and tp == 2 and heads % 4 == 0 and hidden % (4 * LANES) == 0
+        self.split = self.split and depth == sp * LANES
         self.team_bits = TEAM_BITS if self.split else ()
         self.peer_bits = PEER_BITS if self.split else ()
         self.team = 4 if self.split else 1
@@ -74,6 +75,94 @@
     return pl.CostEstimate(
         flops=int(flops), bytes_accessed=int(moved), transcendentals=int(transcendentals)
     )
+
+
+def pack_kernel(plan, heads, me_ref, qn, qb, kn, kb, vn, vb, off_ref, *refs):
+    outs, off_s = refs[: plan.team], refs[plan.team]
+    rows = qb.shape[0]
+    local_heads = heads // plan.team
+    t = plan.member(me_ref[0])
+    wide = jnp.concatenate(
+        [off_ref[...], jnp.zeros((rows, LANES - off_ref.shape[1]), F32)], axis=1
+    )
+    off_s[...] = jnp.transpose(wide)
+
+    def broad(ref, head):
+        return ref[:, pl.ds(pl.multiple_of(head * BROAD_SIZE, BROAD_SIZE), BROAD_SIZE)]
+
+    def narrow(ref, head):
+        if heads == 1:
+            return ref[...]
+        both = ref[:, pl.ds(pl.multiple_of((head // 2) * LANES, LANES), LANES)].astype(F32)
+        return jnp.where(head % 2 == 0, both[:, :NARROW_SIZE], both[:, NARROW_SIZE:]).astype(BF)
+
+    for r in range(plan.team):
+        for h in range(local_heads):
+            head = jnp.bitwise_xor(t, r) * local_heads + h
+            out = outs[r]
+            out[h, pl.ds(0, rows), pl.ds(0, LANES)] = broad(kb, head)
+            out[h, pl.ds(0, rows), pl.ds(LANES, LANES)] = broad(vb, head)
+            out[h, pl.ds(0, rows), pl.ds(2 * LANES, LANES)] = jnp.concatenate(
+                [narrow(kn, head), narrow(vn, head)], axis=1
+            )
+            out[h, pl.ds(0, rows), pl.ds(3 * LANES, LANES)] = broad(qb, head)
+            out[h, pl.ds(0, rows), pl.ds(4 * LANES, LANES)] = jnp.concatenate(
+                [narrow(qn, head), jnp.zeros((rows, NARROW_SIZE), BF)], axis=1
+            )
+            row = jnp.concatenate(
+                [
+                    off_s[pl.ds(2 * head + 1, 1), :],
+                    off_s[pl.ds(2 * head, 1), :],
+                    jnp.zeros((EXTRA - 2, rows), F32),
+                ],
+                axis=0,
+            )
+            high = row.astype(BF)
+            rest = row - high.astype(F32)
+            middle = rest.astype(BF)
+            low = (rest - middle.astype(F32)).astype(BF)
+            blank = jnp.zeros((EXTRA, ALL_LANES - 3 * rows), BF)
+            out[h, pl.ds(rows, EXTRA), :] = jnp.concatenate([high, middle, low, blank], axis=1)
+
+
+def pack(plan, me, heads, *arrays):
+    rows = arrays[0].shape[0]
+    shape = jax.ShapeDtypeStruct((heads // plan.team, rows + EXTRA, ALL_LANES), BF)
+    return pl.pallas_call(
+        functools.partial(pack_kernel, plan, heads),
+        out_shape=[shape] * plan.team,
+        in_specs=[SMEM] + [VMEM] * len(arrays),
+        out_specs=[VMEM] * plan.team,
+        scratch_shapes=[pltpu.VMEM((LANES, rows), F32)],
+        cost_estimate=cost(1e6, 2e6),
+        name="pack",
+    )(me, *arrays)
+
+
+def weights_kernel(plan, me_ref, gate, up, down, *outs):
+    t = plan.member(me_ref[0])
+    units = gate.shape[1] // plan.team
+    band = gate.shape[0]
+    for r in range(plan.team):
+        at = pl.multiple_of(jnp.bitwise_xor(t, r) * units, LANES)
+        outs[r][:, pl.ds(0, units)] = gate[:, pl.ds(at, units)]
+        outs[r][:, pl.ds(units, units)] = up[:, pl.ds(at, units)]
+        for j in range(units // band):
+            start = pl.multiple_of(at + j * band, LANES)
+            outs[r][:, pl.ds(2 * units + j * LANES, LANES)] = down[pl.ds(start, band), :]
+
+
+def pack_weights(plan, me, gate, up, down):
+    band, units = gate.shape[0], gate.shape[1] // plan.team
+    shape = jax.ShapeDtypeStruct((band, 3 * units), BF)
+    return pl.pallas_call(
+        functools.partial(weights_kernel, plan),
+        out_shape=[shape] * plan.team,
+        in_specs=[SMEM] + [VMEM] * 3,
+        out_specs=[VMEM] * plan.team,
+        cost_estimate=cost(1e6, 4e6),
+        name="pack_weights",
+    )(me, gate, up, down)
 
 
 def attention_kernel(plan, me_ref, own_ref, *refs):
@@ -201,9 +290,13 @@
 
 def project_kernel(plan, me_ref, broad_ref, narrow_ref, *refs):
     team = plan.team
-    attended = refs[:team]
-    out_ref, a_s, w_s = refs[team:]
-    local_heads, total, _ = attended[0].shape
+    attended, streams = refs[:team], refs[team : 2 * team]
+    out_ref, a_s, w_s, stream_s = refs[2 * team :]
+    rows, share = streams[0].shape
+    for r in range(team):
+        place = jnp.bitwise_xor(plan.member(me_ref[0]), r)
+        stream_s[pl.ds(pl.multiple_of(place * rows, rows), rows), :] = streams[r][...]
+    local_heads, _, _ = attended[0].shape
     t = plan.member(me_ref[0])
     depth = out_ref.shape[1]
     for r in range(team):
@@ -218,79 +311,85 @@
             w_s[pl.ds(at + LANES + NARROW_SIZE, NARROW_SIZE), :] = narrow_ref[
                 pl.ds(pl.multiple_of(head * NARROW_SIZE, NARROW_SIZE), NARROW_SIZE), :
             ]
-    width = min(512, depth)
+    width = min(512, share)
     for n in range(0, depth, width):
-        out_ref[:, pl.ds(n, width)] = jnp.dot(
-            a_s[...], w_s[:, pl.ds(n, width)], preferred_element_type=F32
-        ).astype(BF)
-
-
-def project(plan, me, attended, out_broad, out_narrow):
+        mine = (me_ref[1] == n // share).astype(F32)
+        part = jnp.dot(a_s[...], w_s[:, pl.ds(n, width)], preferred_element_type=F32)
+        part = part + mine * stream_s[:, pl.ds(n % share, width)].astype(F32)
+        out_ref[:, pl.ds(n, width)] = part.astype(BF)
+
+
+def project(plan, me, attended, streams, out_broad, out_narrow):
     local_heads, total, _ = attended[0].shape
     depth = out_broad.shape[1]
     inner = plan.team * local_heads * 2 * LANES
     return pl.pallas_call(
         functools.partial(project_kernel, plan),
         out_shape=jax.ShapeDtypeStruct((total, depth), BF),
-        in_specs=[SMEM] + [VMEM] * (2 + len(attended)),
+        in_specs=[SMEM] + [VMEM] * (2 + 2 * len(attended)),
         out_specs=VMEM,
-        scratch_shapes=[pltpu.VMEM((total, inner), BF), pltpu.VMEM((inner, depth), BF)],
+        scratch_shapes=[
+            pltpu.VMEM((total, inner), BF),
+            pltpu.VMEM((inner, depth), BF),
+            pltpu.VMEM((total, streams[0].shape[1]), BF),
+        ],
         cost_estimate=cost(2 * total * inner * depth, 2 * total * depth),
         name="project",
-    )(me, out_broad, out_narrow, *attended)
-
-
-def mixer_kernel(plan, gate_parts, down_parts, me_ref, gain_ref, mine_ref, other_ref, *refs):
+    )(me, out_broad, out_narrow, *attended, *streams)
+
+
+def mixer_kernel(plan, weight_parts, me_ref, gain_ref, mine_ref, other_ref, *refs):
     team, tp = plan.team, plan.tp
-    streams = refs[:team]
-    refs = refs[team:]
-    gates, refs = refs[:gate_parts], refs[gate_parts:]
-    downs, refs = refs[:down_parts], refs[down_parts:]
+    weights, refs = refs[:weight_parts], refs[weight_parts:]
     mid_ref, mixed_ref, gu_s, down_s, normed_s, mid_s, gu_sems, down_sems = refs
     me, core = me_ref[0], me_ref[1]
     t = plan.member(me)
-    rows, depth = streams[0].shape
-    band = gu_s.shape[0] // plan.sp
+    total, depth = mine_ref.shape
+    rows = total // team
+    band = depth // plan.sp
     units = down_s.shape[0]
-    column = depth // plan.sp
     gate_copies, down_copies = [], []
     if plan.split:
-        for rw in range(plan.peers):
-            for r in range(team):
-                place = jnp.bitwise_xor(me, plan.index(r, rw))
-                number = rw * team + r
+        for part, (half, rw) in enumerate(WEIGHT_PARTS):
+            for s in range(2):
+                place = pl.multiple_of(
+                    jnp.bitwise_xor(me, plan.index(2 * half + s, rw)) * band, band
+                )
+                number = 2 * part + s
                 gate_copies.append(
                     pltpu.make_async_copy(
-                        gates[rw].at[r],
-                        gu_s.at[pl.ds(pl.multiple_of(place * band, band), band), :],
+                        weights[part].at[s, :, pl.ds(0, 2 * units)],
+                        gu_s.at[pl.ds(place, band), :],
                         gu_sems.at[number],
                     )
                 )
-                down_copies.append(
-                    pltpu.make_async_copy(
-                        downs[rw].at[r],
-                        down_s.at[:, pl.ds(pl.multiple_of(place * column, column), column)],
-                        down_sems.at[number],
+                for j in range(units // band):
+                    down_copies.append(
+                        pltpu.make_async_copy(
+                            weights[part].at[s, :, pl.ds(2 * units + j * band, band)],
+                            down_s.at[pl.ds(j * band, band), pl.ds(place, band)],
+                            down_sems.at[number * (units // band) + j],
+                        )
                     )
-                )
     else:
-        gate_copies.append(pltpu.make_async_copy(gates[0], gu_s, gu_sems.at[0]))
-        down_copies.append(pltpu.make_async_copy(downs[0], down_s, down_sems.at[0]))
+        gate_copies.append(
+            pltpu.make_async_copy(weights[0], gu_s.at[:, pl.ds(0, units)], gu_sems.at[0])
+        )
+        gate_copies.append(
+            pltpu.make_async_copy(weights[1], gu_s.at[:, pl.ds(units, units)], gu_sems.at[1])
+        )
+        down_copies.append(pltpu.make_async_copy(weights[2], down_s, down_sems.at[0]))
     for copy in gate_copies + down_copies:
         copy.start()
-    for r in range(team):
-        at = pl.ds(pl.multiple_of(jnp.bitwise_xor(t, r) * rows, rows), rows)
-        mid = (
-            streams[r][...].astype(F32)
-            + (mine_ref[at, :].astype(F32) + other_ref[at, :].astype(F32))
-        ).astype(BF)
-        if r == 0:
-            mid_s[...] = mid
-        middle = mid.astype(F32)
+    for k in range(team):
+        at = pl.ds(k * rows, rows)
+        middle = (mine_ref[at, :].astype(F32) + other_ref[at, :].astype(F32)).astype(BF)
+        mid_s[at, :] = middle
+        middle = middle.astype(F32)
         scaled = middle * lax.rsqrt(jnp.mean(middle * middle, axis=1, keepdims=True) + norm_eps)
         normed_s[at, :] = (scaled * gain_ref[...]).astype(BF)
     share = rows // tp
-    mid_ref[...] = mid_s[pl.ds(pl.multiple_of(core * share, share), share), :]
+    mid_ref[...] = mid_s[pl.ds(pl.multiple_of(t * rows + core * share, share), share), :]
     for copy in gate_copies:
         copy.wait()
     gate = jnp.dot(normed_s[...], gu_s[:, :units], preferred_element_type=F32)
@@ -308,36 +407,31 @@
                 ]
 
 
-def mixer(plan, place, gain, mine, other, streams, gates, downs):
-    rows, depth = streams[0].shape
-    total = plan.team * rows
-    units = downs[0].shape[-2]
-    share = rows // plan.tp
-    pieces = plan.sp if plan.split else 1
+WEIGHT_PARTS = ((0, 0), (1, 0), (0, 1), (1, 2), (0, 2), (1, 1), (0, 3), (1, 3))
+
+
+def mixer(plan, place, gain, mine, other, units, weights):
+    total, depth = mine.shape
+    share = total // plan.team // plan.tp
     return pl.pallas_call(
-        functools.partial(mixer_kernel, plan, len(gates), len(downs)),
+        functools.partial(mixer_kernel, plan, len(weights)),
         out_shape=(
             jax.ShapeDtypeStruct((share, depth), BF),
             jax.ShapeDtypeStruct((plan.tp, plan.team, share, depth), BF),
         ),
-        in_specs=[SMEM] + [VMEM] * (3 + plan.team) + [ANY] * (len(gates) + len(downs)),
+        in_specs=[SMEM] + [VMEM] * 3 + [ANY] * len(weights),
         out_specs=(VMEM, VMEM),
         scratch_shapes=[
             pltpu.VMEM((depth, 2 * units), BF),
             pltpu.VMEM((units, depth), BF),
             pltpu.VMEM((total, depth), BF),
-            pltpu.VMEM((rows, depth), BF),
-            pltpu.SemaphoreType.DMA((pieces,)),
-            pltpu.SemaphoreType.DMA((pieces,)),
+            pltpu.VMEM((total, depth), BF),
+            pltpu.SemaphoreType.DMA((2 * len(weights),)),
+            pltpu.SemaphoreType.DMA((2 * len(weights) * max(1, units // LANES),)),
         ],
         cost_estimate=cost(6 * total * depth * units, 8 * total * depth),
         name="mixer",
-    )(place, gain, mine, other, *streams, *gates, *downs)
-
-
-def by_head(array, heads):
-    rows = array.shape[0]
-    return jnp.transpose(array.reshape(rows, heads, -1), (1, 0, 2))
+    )(place, gain, mine, other, *weights)
 
 
 def local(
@@ -357,80 +451,102 @@
     up_weight,
     down_weight,
 ):
+    return layer(
+        plan,
+        stream,
+        query_narrow,
+        query_broad,
+        key_narrow,
+        key_broad,
+        value_narrow,
+        value_broad,
+        key_offsets,
+        out_narrow,
+        out_broad,
+        norm_gain,
+        gate_weight,
+        up_weight,
+        down_weight,
+    )
+
+
+def layer(
+    plan,
+    stream,
+    query_narrow,
+    query_broad,
+    key_narrow,
+    key_broad,
+    value_narrow,
+    value_broad,
+    key_offsets,
+    out_narrow,
+    out_broad,
+    norm_gain,
+    gate_weight,
+    up_weight,
+    down_weight,
+):
     team, peers, tp = plan.team, plan.peers, plan.tp
-    rows, depth = stream.shape
+    _, depth = stream.shape
     heads = query_narrow.shape[1] // NARROW_SIZE
     i = lax.axis_index("sp").astype(jnp.int32)
     core = lax.axis_index("tp").astype(jnp.int32)
     t = plan.member(i)
     place = jnp.stack([i, core])
 
-    narrow = functools.partial(by_head, heads=heads)
-    body = jnp.concatenate(
-        [
-            narrow(key_broad),
-            narrow(value_broad),
-            narrow(key_narrow),
-            narrow(value_narrow),
-            narrow(query_broad),
-            narrow(query_narrow),
-            jnp.zeros((heads, rows, NARROW_SIZE), BF),
-        ],
-        axis=2,
+    width = depth // tp
+    stream = lax.dynamic_slice_in_dim(stream, core * width, width, 1)
+    units = gate_weight.shape[1] // team
+    packed = pack(
+        plan,
+        place,
+        heads,
+        query_narrow,
+        query_broad,
+        key_narrow,
+        key_broad,
+        value_narrow,
+        value_broad,
+        key_offsets,
     )
-    high = lax.reduce_precision(key_offsets, 8, 7)
-    middle = lax.reduce_precision(key_offsets - high, 8, 7)
-    low = key_offsets - high - middle
-    pieces = jnp.stack([high, middle, low]).astype(BF).reshape(3, rows, heads, 2)
-    pieces = jnp.transpose(pieces, (2, 3, 0, 1))[:, ::-1].reshape(heads, 2, 3 * rows)
-    tail = jnp.pad(pieces, ((0, 0), (0, EXTRA - 2), (0, ALL_LANES - 3 * rows)))
-    packed = jnp.concatenate([body, tail], axis=1)
-    packed = packed.reshape(team, heads // team, rows + EXTRA, ALL_LANES)
-
-    units = gate_weight.shape[1] // team
-    joined = jnp.concatenate(
-        [
-            jnp.transpose(gate_weight.reshape(-1, team, units), (1, 0, 2)),
-            jnp.transpose(up_weight.reshape(-1, team, units), (1, 0, 2)),
-        ],
-        axis=2,
-    )
-    downs = down_weight.reshape(team, units, -1)
-
     if plan.split:
-        own = [pick(packed, t)]
-        own += [plan.team_swap(pick(packed, t ^ r), r) for r in range(1, team)]
+        own = [packed[0]] + [plan.team_swap(packed[r], r) for r in range(1, team)]
         own = jnp.stack(own)
         keys = own[..., :KV_LANES]
         parts = [plan.peer_swap(keys, r) for r in range(1, peers)]
+        slots = pack_weights(plan, place, gate_weight, up_weight, down_weight)
+        slots = [slots[0]] + [plan.team_swap(slots[r], r) for r in range(1, team)]
         streams = [stream] + [plan.team_swap(stream, r) for r in range(1, team)]
-        gate_own = jnp.stack(
-            [pick(joined, t)] + [plan.team_swap(pick(joined, t ^ r), r) for r in range(1, team)]
-        )
-        down_own = jnp.stack(
-            [pick(downs, t)] + [plan.team_swap(pick(downs, t ^ r), r) for r in range(1, team)]
-        )
-        gates = [gate_own] + [plan.peer_swap(gate_own, r) for r in range(1, peers)]
-        down_parts = [down_own] + [plan.peer_swap(down_own, r) for r in range(1, peers)]
+        left, right = jnp.stack(slots[:2]), jnp.stack(slots[2:])
+        left1 = plan.peer_swap(left, 1)
+        right2 = plan.peer_swap(right, 2)
+        left2 = plan.peer_swap(left, 2)
+        right1 = plan.peer_swap(right, 1)
+        left3 = plan.peer_swap(left1, 2)
+        right3 = plan.peer_swap(right2, 1)
+        weights = [left, right, left1, right2, left2, right1, left3, right3]
     else:
-        own = packed
+        own = jnp.stack(packed)
         keys = own[0, :, :, :KV_LANES]
         parts = [lax.all_gather(keys, "sp", axis=0)]
         streams = [stream]
-        gates = [lax.all_gather(joined[0], "sp", axis=0, tiled=True)]
-        down_parts = [lax.all_gather(downs[0], "sp", axis=1, tiled=True)]
+        weights = [
+            lax.all_gather(gate_weight, "sp", axis=0, tiled=True),
+            lax.all_gather(up_weight, "sp", axis=0, tiled=True),
+            lax.all_gather(down_weight, "sp", axis=1, tiled=True),
+        ]
 
     mine = attention(plan, place, own, parts)
-    attended = [mine] + [plan.team_swap(mine, r) for r in range(1, team)]
-    partial = project(plan, place, attended, out_broad, out_narrow)
+    attended = [mine]
+    attended += [plan.team_swap(mine, r) for r in range(1, team)]
+    partial = project(plan, place, attended, streams, out_broad, out_narrow)
     if tp == 2:
         other = lax.ppermute(partial, "tp", [(0, 1), (1, 0)])
     else:
         summed = lax.psum(partial.astype(F32), "tp")
         partial, other = summed.astype(BF), jnp.zeros_like(partial)
-    mid, mixed = mixer(
-        plan, place, norm_gain.reshape(1, depth), partial, other, streams, gates, down_parts
-    )
+    mid, mixed = mixer(plan, place, norm_gain.reshape(1, depth), partial, other, units, weights)
     sums = pick(mixed, core).astype(F32)
     if tp & (tp - 1) == 0:
         for c in range(1, tp):
@@ -454,13 +570,14 @@
     def whole(*arrays):
         heads = arrays[1].shape[1] // NARROW_SIZE // sizes["tp"]
         hidden = arrays[11].shape[1] // sizes["tp"]
-        plan = Plan(sizes["sp"], sizes["tp"], heads, hidden)
-        return jax.shard_map(
+        plan = Plan(sizes["sp"], sizes["tp"], heads, hidden, arrays[0].shape[1])
+        step = jax.shard_map(
             functools.partial(local, plan),
             mesh=mesh,
             in_specs=placed,
             out_specs=P(("sp", "tp"), None),
             check_vma=False,
-        )(*arrays)
+        )
+        return step(*arrays)
 
     return whole

time: 267 us -> 207 us (0.78)
  the two profiles are of different devices: /device:TPU:24 before, /device:TPU:10 now
where the time goes in v2:
time: 207 us; the launch traced here: 206 us
  waiting for transfers between devices  138 us (67%)
  Pallas kernels  33.1 us (16%)
  starting transfers between devices  25.5 us (12%)
  other arithmetic  5.24 us (3%)
  local copies, waits for them, and re-layouts  4.38 us (2%)
    ppermute x24, waiting for transfers between devices, swap(): return lax.ppermute(array, 'sp', [(i, i ^ offset) for i in range(self.sp)])  135 us
    ppermute x24, starting transfers between devices, swap(): return lax.ppermute(array, 'sp', [(i, i ^ offset) for i in range(self.sp)])  25.4 us
    pallas_call x1, Pallas kernels, attention(): pl.pallas_call(functools.partial(attention_kernel, plan), out_shape=jax.S...  11.3 us
    pallas_call x1, Pallas kernels, mixer(): pl.pallas_call(functools.partial(mixer_kernel, plan, len(weights)), out_s...  10.9 us
    pallas_call x1, Pallas kernels, project(): pl.pallas_call(functools.partial(project_kernel, plan), out_shape=jax.Sha...  6.15 us
  transfers between devices with their start and end apart: 26, of which 19 were waited for; matrix products, arithmetic and copies ran while one was open for 1% of the time, Pallas kernels for 7%

profile of v2, /device:TPU:10, one launch (start us, length us, event | category | flops | bytes accessed | tf_op | source)
XLA Modules:
  0.0 206.4 jit_solution(6839594936382561343)
XLA Ops:
  2.1 2.3 %pack.1 = (bf16[1,136,640]{2,1,0:T(8,128)(2,1)}, bf16[1,136,640]{2,1,0:T(8,128)(2,1)}, bf16[1,136,640]{2,1,0:T(8,128)(2,1)}, bf16[1,136,640]{2,1,0:T(8,128)(2,1)}) custom-call(s32[2]{0:T(128)} %pad_add_fusion.me_ref, bf16[128,256]{1,0:T(8,128)(2,1)} %qn.1, bf16[128,512]{1,0:T(8,128)(2,1)} %qb.1, bf16[128,256]{1,0:T(8,128)(2,1)} %kn.1, bf16[128,512]{1,0:T(8,128)(2,1)} %kb.1, ...), custom_call_target="tpu_custom_call" | custom-call | flops 1000000 | bytes 2000000 | tf_op jit(solution)/shard_map/pack/pallas_call | solution.py:131
  4.8 2.6 %collective-permute-start.1 = (bf16[1,136,640]{2,1,0:T(8,128)(2,1)}, bf16[1,136,640]{2,1,0:T(8,128)(2,1)S(1)}, u32[]{:S(2)}, u32[]{:S(2)}) collective-permute-start(bf16[1,136,640]{2,1,0:T(8,128)(2,1)} %get-tuple-element.17), channel_id=1, source_target_pairs={{0,16},{2,18},{4,20},{6,22},{8,24},{10,26},{12,28},{14,30},{16,0},... | collective-permute-start | bytes 522248 | tf_op jit(solution)/shard_map/ppermute | solution.py:61
  7.9 4.0 %collective-permute-done = bf16[1,136,640]{2,1,0:T(8,128)(2,1)S(1)} collective-permute-done((bf16[1,136,640]{2,1,0:T(8,128)(2,1)}, bf16[1,136,640]{2,1,0:T(8,128)(2,1)S(1)}, u32[]{:S(2)}, u32[]{:S(2)}) %collective-permute-start) | collective-permute-done | bytes 174112 | tf_op jit(solution)/shard_map/ppermute | solution.py:61
  11.9 8.1 %collective-permute-done.1 = bf16[1,136,640]{2,1,0:T(8,128)(2,1)S(1)} collective-permute-done((bf16[1,136,640]{2,1,0:T(8,128)(2,1)}, bf16[1,136,640]{2,1,0:T(8,128)(2,1)S(1)}, u32[]{:S(2)}, u32[]{:S(2)}) %collective-permute-start.1) | collective-permute-done | bytes 174112 | tf_op jit(solution)/shard_map/ppermute | solution.py:61
  19.9 3.2 %collective-permute-done.2 = bf16[1,136,640]{2,1,0:T(8,128)(2,1)S(1)} collective-permute-done((bf16[1,136,640]{2,1,0:T(8,128)(2,1)}, bf16[1,136,640]{2,1,0:T(8,128)(2,1)S(1)}, u32[]{:S(2)}, u32[]{:S(2)}) %collective-permute-start.2) | collective-permute-done | bytes 174112 | tf_op jit(solution)/shard_map/ppermute | solution.py:61
  28.0 1.6 collective-permute-start.11
  29.6 7.3 %collective-permute-done.3.refs_0_ = bf16[4,1,136,384]{3,2,1,0:T(8,128)(2,1)S(1)} collective-permute-done((bf16[4,1,136,384]{3,2,1,0:T(8,128)(2,1)S(1)}, bf16[4,1,136,384]{3,2,1,0:T(8,128)(2,1)S(1)}, u32[]{:S(2)}, u32[]{:S(2)}) %collective-permute-start.3) | collective-permute-done | bytes 417824 | tf_op jit(solution)/shard_map/ppermute | solution.py:61
  36.8 6.1 %collective-permute-done.4.refs_1_ = bf16[4,1,136,384]{3,2,1,0:T(8,128)(2,1)S(1)} collective-permute-done((bf16[4,1,136,384]{3,2,1,0:T(8,128)(2,1)S(1)}, bf16[4,1,136,384]{3,2,1,0:T(8,128)(2,1)S(1)}, u32[]{:S(2)}, u32[]{:S(2)}) %collective-permute-start.4) | collective-permute-done | bytes 417824 | tf_op jit(solution)/shard_map/ppermute | solution.py:61
  42.9 1.6 collective-permute-done.5.refs_2_
  45.3 11.3 %attention.1.refs_0_ = bf16[1,512,256]{2,1,0:T(8,128)(2,1)} custom-call(s32[2]{0:T(128)} %pad_add_fusion.me_ref, bf16[4,1,136,640]{3,2,1,0:T(8,128)(2,1)} %copy-done.1, bf16[4,1,136,384]{3,2,1,0:T(8,128)(2,1)} %copy-done.9, bf16[4,1,136,384]{3,2,1,0:T(8,128)(2,1)} %copy-done.10, bf16[4,1,136,384]{3,2,1,0:T(8,128)(2,1)} %copy-done.11), custom_call_target="tpu_custom_call" | custom-call | flops 1073741824 | bytes 2785280 | tf_op jit(solution)/shard_map/attention/pallas_call | solution.py:273
  56.7 3.1 %collective-permute-start.7 = (bf16[1,512,256]{2,1,0:T(8,128)(2,1)}, bf16[1,512,256]{2,1,0:T(8,128)(2,1)S(1)}, u32[]{:S(2)}, u32[]{:S(2)}) collective-permute-start(bf16[1,512,256]{2,1,0:T(8,128)(2,1)} %attention.1.refs_0_), channel_id=1, source_target_pairs={{0,16},{2,18},{4,20},{6,22},{8,24},{10,26},{12,28},{14,30},{16,0},... | collective-permute-start | bytes 786440 | tf_op jit(solution)/shard_map/ppermute | solution.py:61
  60.2 5.9 %collective-permute-done.6.refs_1_ = bf16[1,512,256]{2,1,0:T(8,128)(2,1)S(1)} collective-permute-done((bf16[1,512,256]{2,1,0:T(8,128)(2,1)}, bf16[1,512,256]{2,1,0:T(8,128)(2,1)S(1)}, u32[]{:S(2)}, u32[]{:S(2)}) %collective-permute-start.6) | collective-permute-done | bytes 262176 | tf_op jit(solution)/shard_map/ppermute | solution.py:61
  66.1 10.9 %collective-permute-done.7.refs_2_ = bf16[1,512,256]{2,1,0:T(8,128)(2,1)S(1)} collective-permute-done((bf16[1,512,256]{2,1,0:T(8,128)(2,1)}, bf16[1,512,256]{2,1,0:T(8,128)(2,1)S(1)}, u32[]{:S(2)}, u32[]{:S(2)}) %collective-permute-start.7) | collective-permute-done | bytes 262176 | tf_op jit(solution)/shard_map/ppermute | solution.py:61
  76.9 4.1 %collective-permute-done.8.refs_3_ = bf16[1,512,256]{2,1,0:T(8,128)(2,1)S(1)} collective-permute-done((bf16[1,512,256]{2,1,0:T(8,128)(2,1)}, bf16[1,512,256]{2,1,0:T(8,128)(2,1)S(1)}, u32[]{:S(2)}, u32[]{:S(2)}) %collective-permute-start.8) | collective-permute-done | bytes 262176 | tf_op jit(solution)/shard_map/ppermute | solution.py:61
  81.8 6.2 %project.1.mine_ref = bf16[512,2048]{1,0:T(8,128)(2,1)} custom-call(s32[2]{0:T(128)} %pad_add_fusion.me_ref, bf16[512,2048]{1,0:T(8,128)(2,1)} %broad_ref.1, bf16[256,2048]{1,0:T(8,128)(2,1)} %narrow_ref.1, bf16[1,512,256]{2,1,0:T(8,128)(2,1)} %attention.1.refs_0_, bf16[1,512,256]{2,1,0:T(8,128)(2,1)} %copy-done.13, bf16[1,512,256]{2,1,0:T(8,128)(2,1)} %copy-done.14, ...), custom_call_target="tpu_custom_call" | custom-call | flops 2147483648 | bytes 2097152 | tf_op jit(solution)/shard_map/project/pallas_call | solution.py:326
  87.9 2.5 %pack_weights.1 = (bf16[128,1152]{1,0:T(8,128)(2,1)}, bf16[128,1152]{1,0:T(8,128)(2,1)}, bf16[128,1152]{1,0:T(8,128)(2,1)}, bf16[128,1152]{1,0:T(8,128)(2,1)}) custom-call(s32[2]{0:T(128)} %pad_add_fusion.me_ref, bf16[128,1536]{1,0:T(8,128)(2,1)} %gate.1, bf16[128,1536]{1,0:T(8,128)(2,1)} %up.1, bf16[1536,128]{1,0:T(8,128)(2,1)} %down.1), custom_call_target="tpu_custom_call" | custom-call | flops 1000000 | bytes 4000000 | tf_op jit(solution)/shard_map/pack_weights/pallas_call | solution.py:158
  90.4 1.7 collective-permute-start.15
  92.1 1.8 collective-permute-start.13
  93.9 18.5 %collective-permute-done.15 = bf16[128,1152]{1,0:T(8,128)(2,1)S(1)} collective-permute-done((bf16[128,1152]{1,0:T(8,128)(2,1)}, bf16[128,1152]{1,0:T(8,128)(2,1)S(1)}, u32[]{:S(2)}, u32[]{:S(2)}) %collective-permute-start.15) | collective-permute-done | bytes 294944 | tf_op jit(solution)/shard_map/ppermute | solution.py:61
  112.4 4.9 %collective-permute-done.14 = bf16[128,1152]{1,0:T(8,128)(2,1)S(1)} collective-permute-done((bf16[128,1152]{1,0:T(8,128)(2,1)}, bf16[128,1152]{1,0:T(8,128)(2,1)S(1)}, u32[]{:S(2)}, u32[]{:S(2)}) %collective-permute-start.14) | collective-permute-done | bytes 294944 | tf_op jit(solution)/shard_map/ppermute | solution.py:61
  117.4 2.3 %collective-permute-start.17 = (bf16[2,128,1152]{2,1,0:T(8,128)(2,1)S(1)}, bf16[2,128,1152]{2,1,0:T(8,128)(2,1)S(1)}, u32[]{:S(2)}, u32[]{:S(2)}) collective-permute-start(bf16[2,128,1152]{2,1,0:T(8,128)(2,1)S(1)} %pad_maximum_fusion.2.refs_1_), channel_id=1, source_target_pairs={{0,4},{2,6},{4,0},{6,2},{8,12},{10,14},{12,8},{14,10},{16,20},{18,... | collective-permute-start | bytes 1769480 | tf_op jit(solution)/shard_map/ppermute | solution.py:61
  123.0 10.9 %collective-permute-done.17.refs_3_ = bf16[2,128,1152]{2,1,0:T(8,128)(2,1)S(1)} collective-permute-done((bf16[2,128,1152]{2,1,0:T(8,128)(2,1)S(1)}, bf16[2,128,1152]{2,1,0:T(8,128)(2,1)S(1)}, u32[]{:S(2)}, u32[]{:S(2)}) %collective-permute-start.17) | collective-permute-done | bytes 589856 | tf_op jit(solution)/shard_map/ppermute | solution.py:61
  134.5 2.5 %collective-permute-done.16.refs_2_ = bf16[2,128,1152]{2,1,0:T(8,128)(2,1)S(1)} collective-permute-done((bf16[2,128,1152]{2,1,0:T(8,128)(2,1)S(1)}, bf16[2,128,1152]{2,1,0:T(8,128)(2,1)S(1)}, u32[]{:S(2)}, u32[]{:S(2)}) %collective-permute-start.16) | collective-permute-done | bytes 589856 | tf_op jit(solution)/shard_map/ppermute | solution.py:61
  137.2 12.5 %collective-permute-done.19.refs_5_ = bf16[2,128,1152]{2,1,0:T(8,128)(2,1)S(1)} collective-permute-done((bf16[2,128,1152]{2,1,0:T(8,128)(2,1)S(1)}, bf16[2,128,1152]{2,1,0:T(8,128)(2,1)S(1)}, u32[]{:S(2)}, u32[]{:S(2)}) %collective-permute-start.19) | collective-permute-done | bytes 589856 | tf_op jit(solution)/shard_map/ppermute | solution.py:61
  149.7 11.6 %collective-permute-done.21.refs_7_ = bf16[2,128,1152]{2,1,0:T(8,128)(2,1)} collective-permute-done((bf16[2,128,1152]{2,1,0:T(8,128)(2,1)S(1)}, bf16[2,128,1152]{2,1,0:T(8,128)(2,1)}, u32[]{:S(2)}, u32[]{:S(2)}) %collective-permute-start.21) | collective-permute-done | bytes 589856 | tf_op jit(solution)/shard_map/ppermute | solution.py:61
  161.3 10.9 %mixer.1 = (bf16[64,2048]{1,0:T(8,128)(2,1)}, bf16[2,4,64,2048]{3,2,1,0:T(8,128)(2,1)}) custom-call(s32[2]{0:T(128)} %pad_add_fusion.me_ref, f32[1,2048]{1,0:T(1,128)} %bitcast.33, bf16[512,2048]{1,0:T(8,128)(2,1)} %project.1.mine_ref, bf16[512,2048]{1,0:T(8,128)(2,1)} %collective-permute-done.12.other_ref, bf16[2,128,1152]{2,1,0:T(8,128)(2,1)} %copy-done.3, ...), custom_call_target="tpu_custom_call" | custom-call | flops 2415919104 | bytes 8388608 | tf_op jit(solution)/shard_map/mixer/pallas_call | solution.py:416
  173.7 2.6 %collective-permute-done.22 = bf16[4,64,2048]{2,1,0:T(8,128)(2,1)S(1)} collective-permute-done((bf16[4,64,2048]{2,1,0:T(8,128)(2,1)S(1)}, bf16[4,64,2048]{2,1,0:T(8,128)(2,1)S(1)}, u32[]{:S(2)}, u32[]{:S(2)}) %collective-permute-start.22) | collective-permute-done | bytes 1048608 | tf_op jit(solution)/shard_map/ppermute | solution.py:553
  176.3 1.6 fusion
  178.0 2.8 %collective-permute-start.23 = (bf16[64,2048]{1,0:T(8,128)(2,1)S(1)}, bf16[64,2048]{1,0:T(8,128)(2,1)S(1)}, u32[]{:S(2)}, u32[]{:S(2)}) collective-permute-start(bf16[64,2048]{1,0:T(8,128)(2,1)S(1)} %get-tuple-element.25), channel_id=1, source_target_pairs={{0,8},{2,10},{4,12},{6,14},{8,0},{10,2},{12,4},{14,6},{16,24},{18,... | collective-permute-start | bytes 786440 | tf_op jit(solution)/shard_map/ppermute | solution.py:61
  182.3 9.2 %collective-permute-done.23 = bf16[64,2048]{1,0:T(8,128)(2,1)S(1)} collective-permute-done((bf16[64,2048]{1,0:T(8,128)(2,1)S(1)}, bf16[64,2048]{1,0:T(8,128)(2,1)S(1)}, u32[]{:S(2)}, u32[]{:S(2)}) %collective-permute-start.23) | collective-permute-done | bytes 262176 | tf_op jit(solution)/shard_map/ppermute | solution.py:61
  191.5 7.9 %collective-permute-done.24 = bf16[64,2048]{1,0:T(8,128)(2,1)S(1)} collective-permute-done((bf16[64,2048]{1,0:T(8,128)(2,1)S(1)}, bf16[64,2048]{1,0:T(8,128)(2,1)S(1)}, u32[]{:S(2)}, u32[]{:S(2)}) %collective-permute-start.24) | collective-permute-done | bytes 262176 | tf_op jit(solution)/shard_map/ppermute | solution.py:61
  199.4 6.2 %collective-permute-done.25 = bf16[64,2048]{1,0:T(8,128)(2,1)S(1)} collective-permute-done((bf16[64,2048]{1,0:T(8,128)(2,1)S(1)}, bf16[64,2048]{1,0:T(8,128)(2,1)S(1)}, u32[]{:S(2)}, u32[]{:S(2)}) %collective-permute-start.25) | collective-permute-done | bytes 262176 | tf_op jit(solution)/shard_map/ppermute | solution.py:61
  (68 shorter events, 17.7 us)
Async XLA Ops:
  0.0 27.8 %copy-start = (bf16[128,2048]{1,0:T(8,128)(2,1)S(1)}, bf16[128,2048]{1,0:T(8,128)(2,1)}, u32[]{:S(2)}) copy-start(bf16[128,2048]{1,0:T(8,128)(2,1)} %param.14) | copy-start | bytes 1572868
  4.4 7.5 %collective-permute-start = (bf16[1,136,640]{2,1,0:T(8,128)(2,1)}, bf16[1,136,640]{2,1,0:T(8,128)(2,1)S(1)}, u32[]{:S(2)}, u32[]{:S(2)}) collective-permute-start(bf16[1,136,640]{2,1,0:T(8,128)(2,1)} %get-tuple-element.16), channel_id=1, source_target_pairs={{0,8},{2,10},{4,12},{6,14},{8,0},{10,2},{12,4},{14,6},{16,24},{18,... | collective-permute-start | bytes 522248 | tf_op jit(solution)/shard_map/ppermute | solution.py:61
  4.8 15.1 %collective-permute-start.1 = (bf16[1,136,640]{2,1,0:T(8,128)(2,1)}, bf16[1,136,640]{2,1,0:T(8,128)(2,1)S(1)}, u32[]{:S(2)}, u32[]{:S(2)}) collective-permute-start(bf16[1,136,640]{2,1,0:T(8,128)(2,1)} %get-tuple-element.17), channel_id=1, source_target_pairs={{0,16},{2,18},{4,20},{6,22},{8,24},{10,26},{12,28},{14,30},{16,0},... | collective-permute-start | bytes 522248 | tf_op jit(solution)/shard_map/ppermute | solution.py:61
  7.4 15.8 %collective-permute-start.2 = (bf16[1,136,640]{2,1,0:T(8,128)(2,1)}, bf16[1,136,640]{2,1,0:T(8,128)(2,1)S(1)}, u32[]{:S(2)}, u32[]{:S(2)}) collective-permute-start(bf16[1,136,640]{2,1,0:T(8,128)(2,1)} %get-tuple-element.18), channel_id=1, source_target_pairs={{0,24},{2,26},{4,28},{6,30},{8,16},{10,18},{12,20},{14,22},{16,8},... | collective-permute-start | bytes 522248 | tf_op jit(solution)/shard_map/ppermute | solution.py:61
  24.3 12.6 %collective-permute-start.3 = (bf16[4,1,136,384]{3,2,1,0:T(8,128)(2,1)S(1)}, bf16[4,1,136,384]{3,2,1,0:T(8,128)(2,1)S(1)}, u32[]{:S(2)}, u32[]{:S(2)}) collective-permute-start(bf16[4,1,136,384]{3,2,1,0:T(8,128)(2,1)S(1)} %slice.4), channel_id=1, source_target_pairs={{0,2},{2,0},{4,6},{6,4},{8,10},{10,8},{12,14},{14,12},{16,18},{18,... | collective-permute-start | bytes 1253384 | tf_op jit(solution)/shard_map/ppermute | solution.py:61
  24.9 18.0 %collective-permute-start.4 = (bf16[4,1,136,384]{3,2,1,0:T(8,128)(2,1)S(1)}, bf16[4,1,136,384]{3,2,1,0:T(8,128)(2,1)S(1)}, u32[]{:S(2)}, u32[]{:S(2)}) collective-permute-start(bf16[4,1,136,384]{3,2,1,0:T(8,128)(2,1)S(1)} %slice.4), channel_id=1, source_target_pairs={{0,4},{2,6},{4,0},{6,2},{8,12},{10,14},{12,8},{14,10},{16,20},{18,... | collective-permute-start | bytes 1253384 | tf_op jit(solution)/shard_map/ppermute | solution.py:61
  26.4 18.1 %collective-permute-start.5 = (bf16[4,1,136,384]{3,2,1,0:T(8,128)(2,1)S(1)}, bf16[4,1,136,384]{3,2,1,0:T(8,128)(2,1)S(1)}, u32[]{:S(2)}, u32[]{:S(2)}) collective-permute-start(bf16[4,1,136,384]{3,2,1,0:T(8,128)(2,1)S(1)} %slice.4), channel_id=1, source_target_pairs={{0,6},{2,4},{4,2},{6,0},{8,14},{10,12},{12,10},{14,8},{16,22},{18,... | collective-permute-start | bytes 1253384 | tf_op jit(solution)/shard_map/ppermute | solution.py:61
  27.8 28.8 %copy-start.4 = (bf16[128,1024]{1,0:T(8,128)(2,1)}, bf16[128,1024]{1,0:T(8,128)(2,1)S(1)}, u32[]{:S(2)}) copy-start(bf16[128,1024]{1,0:T(8,128)(2,1)S(1)} %constant_dynamic-slice_fusion.refs_4_) | copy-start | bytes 786436
  27.8 31.9 %collective-permute-start.10 = (bf16[128,1024]{1,0:T(8,128)(2,1)S(1)}, bf16[128,1024]{1,0:T(8,128)(2,1)S(1)}, u32[]{:S(2)}, u32[]{:S(2)}) collective-permute-start(bf16[128,1024]{1,0:T(8,128)(2,1)S(1)} %constant_dynamic-slice_fusion.refs_4_), channel_id=1, source_target_pairs={{0,16},{2,18},{4,20},{6,22},{8,24},{10,26},{12,28},{14,30},{16,0},... | collective-permute-start | bytes 786440 | tf_op jit(solution)/shard_map/ppermute | solution.py:61
  28.0 32.2 %collective-permute-start.11 = (bf16[128,1024]{1,0:T(8,128)(2,1)S(1)}, bf16[128,1024]{1,0:T(8,128)(2,1)}, u32[]{:S(2)}, u32[]{:S(2)}) collective-permute-start(bf16[128,1024]{1,0:T(8,128)(2,1)S(1)} %constant_dynamic-slice_fusion.refs_4_), channel_id=1, source_target_pairs={{0,24},{2,26},{4,28},{6,30},{8,16},{10,18},{12,20},{14,22},{16,8},... | collective-permute-start | bytes 786440 | tf_op jit(solution)/shard_map/ppermute | solution.py:61
  36.8 23.4 %collective-permute-start.9 = (bf16[128,1024]{1,0:T(8,128)(2,1)S(1)}, bf16[128,1024]{1,0:T(8,128)(2,1)}, u32[]{:S(2)}, u32[]{:S(2)}) collective-permute-start(bf16[128,1024]{1,0:T(8,128)(2,1)S(1)} %constant_dynamic-slice_fusion.refs_4_), channel_id=1, source_target_pairs={{0,8},{2,10},{4,12},{6,14},{8,0},{10,2},{12,4},{14,6},{16,24},{18,... | collective-permute-start | bytes 786440 | tf_op jit(solution)/shard_map/ppermute | solution.py:61
  56.6 9.5 %collective-permute-start.6 = (bf16[1,512,256]{2,1,0:T(8,128)(2,1)}, bf16[1,512,256]{2,1,0:T(8,128)(2,1)S(1)}, u32[]{:S(2)}, u32[]{:S(2)}) collective-permute-start(bf16[1,512,256]{2,1,0:T(8,128)(2,1)} %attention.1.refs_0_), channel_id=1, source_target_pairs={{0,8},{2,10},{4,12},{6,14},{8,0},{10,2},{12,4},{14,6},{16,24},{18,... | collective-permute-start | bytes 786440 | tf_op jit(solution)/shard_map/ppermute | solution.py:61
  56.7 20.2 %collective-permute-start.7 = (bf16[1,512,256]{2,1,0:T(8,128)(2,1)}, bf16[1,512,256]{2,1,0:T(8,128)(2,1)S(1)}, u32[]{:S(2)}, u32[]{:S(2)}) collective-permute-start(bf16[1,512,256]{2,1,0:T(8,128)(2,1)} %attention.1.refs_0_), channel_id=1, source_target_pairs={{0,16},{2,18},{4,20},{6,22},{8,24},{10,26},{12,28},{14,30},{16,0},... | collective-permute-start | bytes 786440 | tf_op jit(solution)/shard_map/ppermute | solution.py:61
  59.8 21.3 %collective-permute-start.8 = (bf16[1,512,256]{2,1,0:T(8,128)(2,1)}, bf16[1,512,256]{2,1,0:T(8,128)(2,1)S(1)}, u32[]{:S(2)}, u32[]{:S(2)}) collective-permute-start(bf16[1,512,256]{2,1,0:T(8,128)(2,1)} %attention.1.refs_0_), channel_id=1, source_target_pairs={{0,24},{2,26},{4,28},{6,30},{8,16},{10,18},{12,20},{14,22},{16,8},... | collective-permute-start | bytes 786440 | tf_op jit(solution)/shard_map/ppermute | solution.py:61
  87.9 73.3 %collective-permute-start.12 = (bf16[512,2048]{1,0:T(8,128)(2,1)}, bf16[512,2048]{1,0:T(8,128)(2,1)}, u32[]{:S(2)}, u32[]{:S(2)}) collective-permute-start(bf16[512,2048]{1,0:T(8,128)(2,1)} %project.1.mine_ref), channel_id=1, source_target_pairs={{0,1},{1,0},{2,3},{3,2},{4,5},{5,4},{6,7},{7,6},{8,9},{9,8},{10,11... | collective-permute-start | bytes 6291464 | tf_op jit(solution)/shard_map/ppermute | solution.py:545
  90.4 22.0 %collective-permute-start.15 = (bf16[128,1152]{1,0:T(8,128)(2,1)}, bf16[128,1152]{1,0:T(8,128)(2,1)S(1)}, u32[]{:S(2)}, u32[]{:S(2)}) collective-permute-start(bf16[128,1152]{1,0:T(8,128)(2,1)} %get-tuple-element.22), channel_id=1, source_target_pairs={{0,24},{2,26},{4,28},{6,30},{8,16},{10,18},{12,20},{14,22},{16,8},... | collective-permute-start | bytes 884744 | tf_op jit(solution)/shard_map/ppermute | solution.py:61
  92.1 25.3 %collective-permute-start.14 = (bf16[128,1152]{1,0:T(8,128)(2,1)}, bf16[128,1152]{1,0:T(8,128)(2,1)S(1)}, u32[]{:S(2)}, u32[]{:S(2)}) collective-permute-start(bf16[128,1152]{1,0:T(8,128)(2,1)} %get-tuple-element.21), channel_id=1, source_target_pairs={{0,16},{2,18},{4,20},{6,22},{8,24},{10,26},{12,28},{14,30},{16,0},... | collective-permute-start | bytes 884744 | tf_op jit(solution)/shard_map/ppermute | solution.py:61
  92.1 27.6 %collective-permute-start.13 = (bf16[128,1152]{1,0:T(8,128)(2,1)}, bf16[128,1152]{1,0:T(8,128)(2,1)S(1)}, u32[]{:S(2)}, u32[]{:S(2)}) collective-permute-start(bf16[128,1152]{1,0:T(8,128)(2,1)} %get-tuple-element.20), channel_id=1, source_target_pairs={{0,8},{2,10},{4,12},{6,14},{8,0},{10,2},{12,4},{14,6},{16,24},{18,... | collective-permute-start | bytes 884744 | tf_op jit(solution)/shard_map/ppermute | solution.py:61
  117.4 43.8 %copy-start.2 = (bf16[2,128,1152]{2,1,0:T(8,128)(2,1)}, bf16[2,128,1152]{2,1,0:T(8,128)(2,1)S(1)}, u32[]{:S(2)}) copy-start(bf16[2,128,1152]{2,1,0:T(8,128)(2,1)S(1)} %pad_maximum_fusion.2.refs_1_) | copy-start | bytes 1769476
  117.4 16.5 %collective-permute-start.17 = (bf16[2,128,1152]{2,1,0:T(8,128)(2,1)S(1)}, bf16[2,128,1152]{2,1,0:T(8,128)(2,1)S(1)}, u32[]{:S(2)}, u32[]{:S(2)}) collective-permute-start(bf16[2,128,1152]{2,1,0:T(8,128)(2,1)S(1)} %pad_maximum_fusion.2.refs_1_), channel_id=1, source_target_pairs={{0,4},{2,6},{4,0},{6,2},{8,12},{10,14},{12,8},{14,10},{16,20},{18,... | collective-permute-start | bytes 1769480 | tf_op jit(solution)/shard_map/ppermute | solution.py:61
  120.8 40.5 %copy-start.3 = (bf16[2,128,1152]{2,1,0:T(8,128)(2,1)}, bf16[2,128,1152]{2,1,0:T(8,128)(2,1)S(1)}, u32[]{:S(2)}) copy-start(bf16[2,128,1152]{2,1,0:T(8,128)(2,1)S(1)} %pad_maximum_fusion.1.refs_0_) | copy-start | bytes 1769476
  120.8 16.3 %collective-permute-start.16 = (bf16[2,128,1152]{2,1,0:T(8,128)(2,1)S(1)}, bf16[2,128,1152]{2,1,0:T(8,128)(2,1)S(1)}, u32[]{:S(2)}, u32[]{:S(2)}) collective-permute-start(bf16[2,128,1152]{2,1,0:T(8,128)(2,1)S(1)} %pad_maximum_fusion.1.refs_0_), channel_id=1, source_target_pairs={{0,2},{2,0},{4,6},{6,4},{8,10},{10,8},{12,14},{14,12},{16,18},{18,... | collective-permute-start | bytes 1769480 | tf_op jit(solution)/shard_map/ppermute | solution.py:61
  121.4 28.3 %collective-permute-start.19 = (bf16[2,128,1152]{2,1,0:T(8,128)(2,1)S(1)}, bf16[2,128,1152]{2,1,0:T(8,128)(2,1)S(1)}, u32[]{:S(2)}, u32[]{:S(2)}) collective-permute-start(bf16[2,128,1152]{2,1,0:T(8,128)(2,1)S(1)} %pad_maximum_fusion.2.refs_1_), channel_id=1, source_target_pairs={{0,2},{2,0},{4,6},{6,4},{8,10},{10,8},{12,14},{14,12},{16,18},{18,... | collective-permute-start | bytes 1769480 | tf_op jit(solution)/shard_map/ppermute | solution.py:61
  122.9 26.8 %collective-permute-start.18 = (bf16[2,128,1152]{2,1,0:T(8,128)(2,1)S(1)}, bf16[2,128,1152]{2,1,0:T(8,128)(2,1)}, u32[]{:S(2)}, u32[]{:S(2)}) collective-permute-start(bf16[2,128,1152]{2,1,0:T(8,128)(2,1)S(1)} %pad_maximum_fusion.1.refs_0_), channel_id=1, source_target_pairs={{0,4},{2,6},{4,0},{6,2},{8,12},{10,14},{12,8},{14,10},{16,20},{18,... | collective-permute-start | bytes 1769480 | tf_op jit(solution)/shard_map/ppermute | solution.py:61
  133.9 27.4 %copy-start.6 = (bf16[2,128,1152]{2,1,0:T(8,128)(2,1)}, bf16[2,128,1152]{2,1,0:T(8,128)(2,1)S(1)}, u32[]{:S(2)}) copy-start(bf16[2,128,1152]{2,1,0:T(8,128)(2,1)S(1)} %collective-permute-done.17.refs_3_) | copy-start | bytes 1769476
  133.9 27.3 %collective-permute-start.21 = (bf16[2,128,1152]{2,1,0:T(8,128)(2,1)S(1)}, bf16[2,128,1152]{2,1,0:T(8,128)(2,1)}, u32[]{:S(2)}, u32[]{:S(2)}) collective-permute-start(bf16[2,128,1152]{2,1,0:T(8,128)(2,1)S(1)} %collective-permute-done.17.refs_3_), channel_id=1, source_target_pairs={{0,2},{2,0},{4,6},{6,4},{8,10},{10,8},{12,14},{14,12},{16,18},{18,... | collective-permute-start | bytes 1769480 | tf_op jit(solution)/shard_map/ppermute | solution.py:61
  137.0 24.2 %collective-permute-start.20 = (bf16[2,128,1152]{2,1,0:T(8,128)(2,1)S(1)}, bf16[2,128,1152]{2,1,0:T(8,128)(2,1)}, u32[]{:S(2)}, u32[]{:S(2)}) collective-permute-start(bf16[2,128,1152]{2,1,0:T(8,128)(2,1)S(1)} %collective-permute-done.16.refs_2_), channel_id=1, source_target_pairs={{0,4},{2,6},{4,0},{6,2},{8,12},{10,14},{12,8},{14,10},{16,20},{18,... | collective-permute-start | bytes 1769480 | tf_op jit(solution)/shard_map/ppermute | solution.py:61
  173.5 2.7 %collective-permute-start.22 = (bf16[4,64,2048]{2,1,0:T(8,128)(2,1)S(1)}, bf16[4,64,2048]{2,1,0:T(8,128)(2,1)S(1)}, u32[]{:S(2)}, u32[]{:S(2)}) collective-permute-start(bf16[4,64,2048]{2,1,0:T(8,128)(2,1)S(1)} %dynamic-slice_bitcast_fusion), channel_id=1, source_target_pairs={{0,1},{1,0},{2,3},{3,2},{4,5},{5,4},{6,7},{7,6},{8,9},{9,8},{10,11... | collective-permute-start | bytes 3145736 | tf_op jit(solution)/shard_map/ppermute | solution.py:553
  173.6 31.9 %copy-start.5 = (bf16[64,2048]{1,0:T(8,128)(2,1)S(1)}, bf16[64,2048]{1,0:T(8,128)(2,1)}, u32[]{:S(2)}) copy-start(bf16[64,2048]{1,0:T(8,128)(2,1)} %get-tuple-element.23) | copy-start | bytes 786436
  178.0 13.5 %collective-permute-start.23 = (bf16[64,2048]{1,0:T(8,128)(2,1)S(1)}, bf16[64,2048]{1,0:T(8,128)(2,1)S(1)}, u32[]{:S(2)}, u32[]{:S(2)}) collective-permute-start(bf16[64,2048]{1,0:T(8,128)(2,1)S(1)} %get-tuple-element.25), channel_id=1, source_target_pairs={{0,8},{2,10},{4,12},{6,14},{8,0},{10,2},{12,4},{14,6},{16,24},{18,... | collective-permute-start | bytes 786440 | tf_op jit(solution)/shard_map/ppermute | solution.py:61
  180.8 18.6 %collective-permute-start.24 = (bf16[64,2048]{1,0:T(8,128)(2,1)S(1)}, bf16[64,2048]{1,0:T(8,128)(2,1)S(1)}, u32[]{:S(2)}, u32[]{:S(2)}) collective-permute-start(bf16[64,2048]{1,0:T(8,128)(2,1)S(1)} %get-tuple-element.27), channel_id=1, source_target_pairs={{0,16},{2,18},{4,20},{6,22},{8,24},{10,26},{12,28},{14,30},{16,0},... | collective-permute-start | bytes 786440 | tf_op jit(solution)/shard_map/ppermute | solution.py:61
  181.4 24.2 %collective-permute-start.25 = (bf16[64,2048]{1,0:T(8,128)(2,1)S(1)}, bf16[64,2048]{1,0:T(8,128)(2,1)S(1)}, u32[]{:S(2)}, u32[]{:S(2)}) collective-permute-start(bf16[64,2048]{1,0:T(8,128)(2,1)S(1)} %get-tuple-element.26), channel_id=1, source_target_pairs={{0,24},{2,26},{4,28},{6,30},{8,16},{10,18},{12,20},{14,22},{16,8},... | collective-permute-start | bytes 786440 | tf_op jit(solution)/shard_map/ppermute | solution.py:61
  (10 other events, 107.4 us)
